TPU v7x, 128 devices: a whole 4x4x4 slice. The times are simulated.
128 devices in a mesh: rep: 2 (over x_hi), fs: 4 (over x_lo, core), tp: 16 (over z, y).
Axes of the slice: x: 4 (x_hi: 2, x_lo: 2; x = x_hi * 2 + x_lo), y: 4, z: 4, core: 2. Of those that a mesh axis runs over, the one named last changes fastest.
Arguments:
- inputs: bfloat16 [4096, 4096], P(('rep', 'fs', 'tp')), may hold values from -6 to 6
- w_gate: bfloat16 [4096, 11008], P('fs', 'tp'), may hold values from -0.09375 to 0.09375
- w_up: bfloat16 [4096, 11008], P('fs', 'tp'), may hold values from -0.09375 to 0.09375
- w_down: bfloat16 [11008, 4096], P('tp', 'fs'), may hold values from -0.0546875 to 0.0546875
- d_out: bfloat16 [4096, 4096], P(('rep', 'fs', 'tp')), may hold values from -24 to 24
Outputs:
- grad_inputs: bfloat16 [4096, 4096], P(('rep', 'fs', 'tp'))
- grad_gate: float32 [4096, 11008], P('fs', 'tp')
- grad_up: float32 [4096, 11008], P('fs', 'tp')
- grad_down: float32 [11008, 4096], P('tp', 'fs')
All inputs are finite; a program needn't handle non-finite values.
Results may differ from a plain program's by a relative error of at most 0.00185.
Values may be sent and summed in bfloat16 or wider, within the bound.
No kernel may reach another device: no remote copies, remote signals or barrier semaphores. Data moves between devices by JAX's collectives and lax.ppermute only.
A program may use at most 192 MiB of HBM per device.

v0:
```python
import functools

import jax
import jax.numpy as jnp
from jax import lax
from jax.experimental import pallas as pl
from jax.experimental.pallas import tpu as pltpu
from jax.sharding import PartitionSpec as P


AXES = ("rep", "fs", "tp")
BF, F32, F16 = jnp.bfloat16, jnp.float32, jnp.float16
W_MAX = 0.09375
ANY = pl.BlockSpec(memory_space=pl.ANY)
VMEM = pl.BlockSpec(memory_space=pltpu.VMEM)
LIMIT = 56 * 1024 * 1024

ROWS, DEPTH, UNITS = 32, 1024, 688
TOK, WIDE = 16 * ROWS, 4 * DEPTH
CUT = 336
LOW = 1040
TAIL = 128


def index_of(x, c, z, y):
    x, z, y = x % 4, z % 4, y % 4
    return (x // 2) * 64 + ((x % 2) * 2 + c) * 16 + z * 4 + y


def moved(array, dx=0, flip=0, dz=0, dy=0):
    pairs = []
    for x in range(4):
        for c in range(2):
            for z in range(4):
                for y in range(4):
                    pairs.append((index_of(x + dx, c ^ flip, z + dz, y + dy), index_of(x, c, z, y)))
    return lax.ppermute(array, AXES, pairs)


def dot(a, b, ca, cb):
    return lax.dot_general(a, b, (((ca,), (cb,)), ((), ())), preferred_element_type=F32)


def place():
    tp = lax.axis_index("tp")
    return tp // 4, tp % 4


def call(body, out_shape, scratch, flops, ins, outs, args, nbytes):
    return pl.pallas_call(
        body,
        out_shape=out_shape,
        in_specs=ins,
        out_specs=outs,
        scratch_shapes=scratch,
        compiler_params=pltpu.CompilerParams(vmem_limit_bytes=LIMIT),
        cost_estimate=pl.CostEstimate(flops=flops, bytes_accessed=nbytes, transcendentals=0),
    )(*args)


D_FROM = ((0, 0, 4, 0), (1, 0, 4, 1), (2, 0, 4, 3), (3, 0, 2, 2), (4, 2, 2, 2))


def forward_kernel(*refs):
    x_in, ds, was, wbs = refs[0], refs[1:6], refs[6:10], refs[10:14]
    acts, side, x_own, d_own = refs[14:18]
    x, d, wa, wb, gate, up, back, act, sx, sd, sw, so = refs[18:]
    z, y = place()
    d_copies = []
    for i, first, count, off in D_FROM:
        for j in range(count):
            row = pl.multiple_of((lax.rem(z + off, 4) * 4 + lax.rem(y + first + j, 4)) * ROWS, ROWS)
            d_copies.append(
                pltpu.make_async_copy(ds[i].at[pl.ds(j * ROWS, ROWS)], d.at[pl.ds(row, ROWS)], sd.at[len(d_copies)]))
    x_copies = [
        pltpu.make_async_copy(x_in.at[:, pl.ds(k * DEPTH, DEPTH)], x.at[:, pl.ds(k * DEPTH, DEPTH)], sx.at[k])
        for k in range(4)
    ]
    w_copies = [
        (pltpu.make_async_copy(was[k], wa.at[k], sw.at[2 * k]), pltpu.make_async_copy(wbs[k], wb.at[k], sw.at[2 * k + 1]))
        for k in range(4)
    ]
    for c in (x_copies[0], *w_copies[0], *d_copies):
        c.start()
    for k in range(1, 4):
        for c in (x_copies[k], *w_copies[k]):
            c.start()
    outs = []
    for k in range(4):
        for c in (x_copies[k], *w_copies[k]):
            c.wait()

        def first(j, _):
            t = pl.ds(pl.multiple_of(j * 256, 256), 256)
            xk = x[t, k * DEPTH:(k + 1) * DEPTH]
            for into, w in ((gate, wa), (up, wb)):
                part = dot(w[k, :UNITS], xk, 1, 1)
                into[:, t] = part if k == 0 else into[:, t] + part
            return 0

        def second(j, _):
            t = pl.ds(pl.multiple_of(j * 256, 256), 256)
            dk = d[t, k * DEPTH:(k + 1) * DEPTH]
            for rows, w in ((slice(0, CUT), wa), (slice(CUT, UNITS), wb)):
                part = dot(w[k, UNITS:], dk, 1, 1)
                back[rows, t] = part if k == 0 else back[rows, t] + part
            return 0

        lax.fori_loop(0, 2, first, 0)
        if k == 0:
            for c in d_copies:
                c.wait()
        lax.fori_loop(0, 2, second, 0)
        if k == 1:
            for i, (v, to) in enumerate(((x, x_own), (d, d_own))):
                outs.append(pltpu.make_async_copy(v.at[:, pl.ds(0, DEPTH)], to, so.at[i]))
                for h in range(2):
                    outs.append(pltpu.make_async_copy(
                        v.at[:, pl.ds(DEPTH + h * TOK, TOK)],
                        side.at[pl.ds(3 * UNITS + (2 * i + h) * TOK, TOK)], so.at[2 + 2 * i + h]))
            for c in outs:
                c.start()

    def unit(i, _):
        r = pl.ds(pl.multiple_of(i * 16, 16), 16)
        g = gate[r, :].astype(BF).astype(F32)
        u = up[r, :].astype(BF).astype(F32)
        b = back[r, :].astype(BF).astype(F32)
        sigma = 1.0 / (1.0 + jnp.exp(-g))
        active = g * sigma
        act[r, :] = (b * u * sigma * (1.0 + g * (1.0 - sigma))).astype(BF)
        act[pl.ds(pl.multiple_of(UNITS + i * 16, 16), 16), :] = (b * active).astype(BF)
        act[pl.ds(pl.multiple_of(2 * UNITS + i * 16, 16), 16), :] = (active * u).astype(BF)
        return 0

    lax.fori_loop(0, UNITS // 16, unit, 0)
    outs.append(pltpu.make_async_copy(act, acts, so.at[6]))
    outs.append(pltpu.make_async_copy(act, side.at[pl.ds(0, 3 * UNITS)], so.at[7]))
    for c in outs[-2:]:
        c.start()
    for c in outs:
        c.wait()


def forward(x, ds, was, wbs):
    shape = jax.ShapeDtypeStruct
    return call(
        forward_kernel,
        (shape((3 * UNITS, TOK), BF), shape((3 * UNITS + 4 * TOK, TOK), BF), shape((TOK, DEPTH), BF), shape((TOK, DEPTH), BF)),
        [
            pltpu.VMEM((TOK, WIDE), BF), pltpu.VMEM((TOK, WIDE), BF),
            pltpu.VMEM((4, UNITS + CUT, DEPTH), BF), pltpu.VMEM((4, 2 * UNITS - CUT, DEPTH), BF),
            pltpu.VMEM((UNITS, TOK), F32), pltpu.VMEM((UNITS, TOK), F32), pltpu.VMEM((UNITS, TOK), F32),
            pltpu.VMEM((3 * UNITS, TOK), BF),
            pltpu.SemaphoreType.DMA((4,)), pltpu.SemaphoreType.DMA((16,)),
            pltpu.SemaphoreType.DMA((8,)), pltpu.SemaphoreType.DMA((8,)),
        ],
        2 * TOK * WIDE * UNITS * 3,
        [ANY] * 14,
        (ANY,) * 4,
        (x, *ds, *was, *wbs),
        34 << 20,
    )


def input_kernel(*refs):
    acts, was, wbs, out = refs[0], refs[1:5], refs[5:9], refs[9]
    wa, wb, tg, tu, scale, sw = refs[10:]
    copies = [
        (pltpu.make_async_copy(was[k].at[pl.ds(0, UNITS)], wa.at[k], sw.at[2 * k]),
         pltpu.make_async_copy(wbs[k].at[pl.ds(0, UNITS)], wb.at[k], sw.at[2 * k + 1]))
        for k in range(4)
    ]
    for pair in copies:
        for c in pair:
            c.start()
    tg[...] = acts[:UNITS, :].T
    tu[...] = acts[UNITS:2 * UNITS, :].T
    norm = jnp.sum(jnp.abs(tg[...].astype(F32)), axis=1, keepdims=True)
    norm = norm + jnp.sum(jnp.abs(tu[...].astype(F32)), axis=1, keepdims=True)
    e = jnp.ceil(jnp.log2(jnp.maximum(norm * (1.02 * W_MAX), 1e-30)))
    scale[...] = jnp.broadcast_to(jnp.exp2(14.0 - e), (TOK, TAIL))
    out[:, WIDE:] = jnp.broadcast_to(e, (TOK, TAIL))
    for k in range(4):
        for c in copies[k]:
            c.wait()

        def tile(j, _):
            n = pl.ds(pl.multiple_of(j * 256, 256), 256)
            m = pl.ds(pl.multiple_of(k * DEPTH + j * 256, 256), 256)
            v = dot(tg[...], wa[k, :, n], 1, 0) + dot(tu[...], wb[k, :, n], 1, 0)
            out[:, m] = v * scale[:, :1]
            return 0

        lax.fori_loop(0, DEPTH // 256, tile, 0)


def input_sums(acts, was, wbs):
    return call(
        input_kernel,
        jax.ShapeDtypeStruct((TOK, WIDE + TAIL), F32),
        [
            pltpu.VMEM((4, UNITS, DEPTH), BF), pltpu.VMEM((4, UNITS, DEPTH), BF),
            pltpu.VMEM((TOK, UNITS), BF), pltpu.VMEM((TOK, UNITS), BF),
            pltpu.VMEM((TOK, TAIL), F32),
            pltpu.SemaphoreType.DMA((8,)),
        ],
        2 * TOK * WIDE * UNITS * 2,
        [VMEM] + [ANY] * 8,
        VMEM,
        (acts, *was, *wbs),
        22 << 20,
    )


def weight_kernel(picks, has_base, n_in, *refs):
    ins, outs = refs[:n_in], refs[n_in:n_in + 3]
    a, xc, dc, total, sa, sc, sb, so = refs[n_in + 3:]
    copies_a, copies_x, copies_d = [], [], []
    n = 0
    for g, (pieces, x_at, d_at) in enumerate(picks):
        for i, r0, r1 in pieces:
            copies_a.append(pltpu.make_async_copy(
                ins[i].at[pl.ds(0, r1 - r0)], a.at[pl.ds(r0, r1 - r0), pl.ds(g * TOK, TOK)], sa.at[n]))
            n += 1
        for (i, sub), buf, into, half in ((x_at, xc, copies_x, 0), (d_at, dc, copies_d, 1)):
            if len(ins[i].shape) == 4:
                pairs = [(ins[i].at[:, sub], buf.at[g])]
            elif sub is None:
                pairs = [(ins[i], buf.at[g])]
            else:
                pairs = [(ins[i].at[pl.ds(sub + h * TOK, TOK)], buf.at[g, :, pl.ds(h * TOK, TOK)]) for h in range(2)]
            for h, (src, to) in enumerate(pairs):
                into.append(pltpu.make_async_copy(src, to, sc.at[4 * g + 2 * half + h]))
    base = []
    if has_base:
        base = [pltpu.make_async_copy(ins[n_in - 3 + i], total.at[i], sb.at[i]) for i in range(3)]
    for c in copies_a + copies_x + copies_d + base:
        c.start()
    for c in copies_a + copies_x:
        c.wait()
    done = []
    for i in range(3):
        if i == 2:
            for c in copies_d:
                c.wait()
        if has_base:
            base[i].wait()
        cols = dc if i == 2 else xc

        def tile(j, _):
            m = pl.ds(pl.multiple_of(j * 256, 256), 256)
            depth = len(picks) * TOK
            v = dot(a[i * UNITS:(i + 1) * UNITS, :], cols[..., m].reshape(depth, 256), 1, 0)
            total[i, :, m] = total[i, :, m] + v if has_base else v
            return 0

        lax.fori_loop(0, DEPTH // 256, tile, 0)
        done.append(pltpu.make_async_copy(total.at[i], outs[i], so.at[i]))
        done[-1].start()
    for c in done:
        c.wait()


def weight_sums(groups, base):
    ins, picks = [], []

    def slot(v):
        for i, w in enumerate(ins):
            if w is v:
                return i
        ins.append(v)
        return len(ins) - 1

    n_pieces = 0
    tiled = groups[0][2][0].ndim == 4
    for pieces, rows, (xv, xi), (dv, di) in groups:
        row, marks = 0, []
        for p, m in zip(pieces, rows):
            marks.append((slot(p), row, row + m))
            row += m
            n_pieces += 1
        picks.append((marks, (slot(xv), xi), (slot(dv), di)))
    ins += list(base or [])
    n = len(groups)
    col = (n, 16, ROWS, DEPTH) if tiled else (n, TOK, DEPTH)
    out = jax.ShapeDtypeStruct((UNITS, DEPTH), F32)
    return call(
        functools.partial(weight_kernel, picks, base is not None, len(ins)),
        (out,) * 3,
        [
            pltpu.VMEM((3 * UNITS, n * TOK), BF), pltpu.VMEM(col, BF), pltpu.VMEM(col, BF),
            pltpu.VMEM((3, UNITS, DEPTH), F32),
            pltpu.SemaphoreType.DMA((n_pieces,)), pltpu.SemaphoreType.DMA((4 * n,)),
            pltpu.SemaphoreType.DMA((3,)), pltpu.SemaphoreType.DMA((3,)),
        ],
        2 * 3 * UNITS * DEPTH * n * TOK,
        [ANY] * len(ins),
        (ANY,) * 3,
        ins,
        n * (4 << 20) + (16 << 20),
    )


def block(inputs, w_gate, w_up, w_down, d_out):
    fs = lax.axis_index("fs")

    def relative(v):
        parts = [v[:, i * DEPTH:(i + 1) * DEPTH] for i in range(4)]
        out = []
        for k in range(4):
            w = parts[k]
            for f in range(1, 4):
                w = jnp.where(fs == f, parts[f ^ k], w)
            out.append(w)
        return out

    xp, dp = relative(inputs), relative(d_out)
    x_own, d_own = jnp.concatenate(xp, axis=1), jnp.concatenate(dp, axis=1)

    x = lax.all_gather(x_own, "tp", axis=0, tiled=True)
    line = jnp.concatenate([d_own] + [moved(d_own, dy=d) for d in (1, 2, 3)], axis=0)
    up, down = moved(line, dz=1), moved(line, dz=-1)
    h = 2 * ROWS
    ds = (line, up, down, moved(up[:h], dz=1), moved(down[h:], dz=-1))

    side = moved(jnp.stack([xp[1], dp[1], xp[3], dp[3]]), flip=1)
    far = jnp.stack([xp[0], side[0], dp[0], side[1]])
    near = jnp.stack([xp[2], side[2], dp[2], side[3]])
    got = jnp.stack([moved(near, dx=1), moved(near, dx=-1), moved(far, dx=2)])
    cols = lax.all_gather(got.reshape(12, ROWS, DEPTH), "tp", axis=0)

    wa = jnp.concatenate([w_gate.T, w_down[:CUT]], axis=0)
    wb = jnp.concatenate([w_up.T, w_down[CUT:]], axis=0)
    wa2, wb2 = moved(wa, dx=1), moved(wb, dx=-1)
    wa1, wb1 = moved(wa, flip=1), moved(wb, flip=1)
    wa3, wb3 = moved(wa2, flip=1), moved(wb2, flip=1)
    was, wbs = (wa, wa1, wa2, wa3), (wb, wb1, wb2, wb3)

    acts, side, x_cols, d_cols = forward(x, ds, was, wbs)

    am, ap = moved(acts, dx=1), moved(acts, dx=-1)
    side = moved(side, flip=1)
    oa, ob = moved(am[:LOW], dx=1), moved(ap[LOW:], dx=-1)
    sm, sp = moved(am, flip=1), moved(ap, flip=1)
    soa, sob = moved(oa, flip=1), moved(ob, flip=1)

    packed = input_sums(acts, was, wbs).astype(F16)
    got = lax.all_to_all(packed, "tp", 0, 0, tiled=True)
    got = got.reshape(16, ROWS, WIDE + TAIL).astype(F32)
    back = jnp.exp2(got[:, :, WIDE:WIDE + 1] - 14.0)
    grad_inputs = jnp.sum(got[:, :, :WIDE] * back, axis=0).astype(BF)
    grad_inputs = jnp.concatenate(relative(grad_inputs), axis=1)

    full, cut = (3 * UNITS,), (LOW, 3 * UNITS - LOW)
    at = 3 * UNITS
    sums = weight_sums(
        [([acts], full, (x_cols, None), (d_cols, None)), ([side], full, (side, at), (side, at + 2 * TOK))], None)
    sums = weight_sums(
        [([am], full, (cols, 0), (cols, 2)), ([sm], full, (cols, 1), (cols, 3)),
         ([ap], full, (cols, 4), (cols, 6)), ([sp], full, (cols, 5), (cols, 7))], sums)
    sums = weight_sums(
        [([oa, ob], cut, (cols, 8), (cols, 10)), ([soa, sob], cut, (cols, 9), (cols, 11))], sums)
    return grad_inputs, sums[0].T, sums[1].T, sums[2]


def solution(mesh):
    tok = P(AXES, None)
    return jax.shard_map(
        block,
        mesh=mesh,
        in_specs=(tok, P("fs", "tp"), P("fs", "tp"), P("tp", "fs"), tok),
        out_specs=(tok, P("fs", "tp"), P("fs", "tp"), P("tp", "fs")),
        check_vma=False,
    )
```

profile of v0, /device:TPU:1, one launch (start us, length us, event | category | flops | bytes accessed | tf_op | source)
XLA Modules:
  0.0 422.3 jit_solution(12555957587919463247)
XLA Ops:
  18.4 3.4 collective-permute-done.20
  21.8 6.3 %collective-permute-done.19 = bf16[4,32,1024]{2,1,0:T(8,128)(2,1)S(1)} collective-permute-done((bf16[4,32,1024]{2,1,0:T(8,128)(2,1)S(1)}, bf16[4,32,1024]{2,1,0:T(8,128)(2,1)S(1)}, u32[]{:S(2)}, u32[]{:S(2)}) %collective-permute-start.19) | collective-permute-done | bytes 262176 | tf_op jit(solution)/shard_map/ppermute | solution.py:37
  38.3 3.5 collective-permute-done.2
  41.8 6.7 %collective-permute-done.1 = bf16[32,4096]{1,0:T(8,128)(2,1)S(1)} collective-permute-done((bf16[32,4096]{1,0:T(8,128)(2,1)S(1)}, bf16[32,4096]{1,0:T(8,128)(2,1)S(1)}, u32[]{:S(2)}, u32[]{:S(2)}) %collective-permute-start.1) | collective-permute-done | bytes 262176 | tf_op jit(solution)/shard_map/ppermute | solution.py:37
  54.0 26.7 %collective-permute-done.11.refs_12_.refs_7_ = bf16[1040,1024]{1,0:T(8,128)(2,1)S(1)} collective-permute-done((bf16[1040,1024]{1,0:T(8,128)(2,1)S(1)}, bf16[1040,1024]{1,0:T(8,128)(2,1)S(1)}, u32[]{:S(2)}, u32[]{:S(2)}) %collective-permute-start.11) | collective-permute-done | bytes 2129952 | tf_op jit(solution)/shard_map/ppermute | solution.py:37
  82.3 3.9 collective-permute-start.3
  89.5 31.7 %collective-permute-done.3.refs_2_ = bf16[128,4096]{1,0:T(8,128)(2,1)S(1)} collective-permute-done((bf16[128,4096]{1,0:T(8,128)(2,1)S(1)}, bf16[128,4096]{1,0:T(8,128)(2,1)S(1)}, u32[]{:S(2)}, u32[]{:S(2)}) %collective-permute-start.3) | collective-permute-done | bytes 1048608 | tf_op jit(solution)/shard_map/ppermute | solution.py:37
  121.8 18.9 %collective-permute-done.6.refs_5_ = bf16[64,4096]{1,0:T(8,128)(2,1)S(1)} collective-permute-done((bf16[64,4096]{1,0:T(8,128)(2,1)S(1)}, bf16[64,4096]{1,0:T(8,128)(2,1)S(1)}, u32[]{:S(2)}, u32[]{:S(2)}) %collective-permute-start.6) | collective-permute-done | bytes 524320 | tf_op jit(solution)/shard_map/ppermute | solution.py:37
  142.5 22.3 %collective-permute-done.5.refs_4_ = bf16[64,4096]{1,0:T(8,128)(2,1)S(1)} collective-permute-done((bf16[64,4096]{1,0:T(8,128)(2,1)S(1)}, bf16[64,4096]{1,0:T(8,128)(2,1)S(1)}, u32[]{:S(2)}, u32[]{:S(2)}) %collective-permute-start.5) | collective-permute-done | bytes 524320 | tf_op jit(solution)/shard_map/ppermute | solution.py:37
  168.3 21.4 %shard_map.84 = (bf16[2064,512]{1,0:T(8,128)(2,1)}, bf16[4112,512]{1,0:T(8,128)(2,1)}, bf16[512,1024]{1,0:T(8,128)(2,1)}, bf16[512,1024]{1,0:T(8,128)(2,1)}) custom-call(bf16[512,4096]{1,0:T(8,128)(2,1)} %all-gather.3.cloned.1.call-done.refs_0_, bf16[128,4096]{1,0:T(8,128)(2,1)} %copy-done.12, bf16[128,4096]{1,0:T(8,128)(2,1)} %copy-done.14, ...), custom_call_target="tpu_custom_call" | custom-call | flops 8657043456 | bytes 35651584 | tf_op jit(solution)/shard_map/pallas_call | solution.py:50
  189.7 16.2 %shard_map.85 = f32[512,4224]{1,0:T(8,128)} custom-call(bf16[2064,512]{1,0:T(8,128)(2,1)} %get-tuple-element.17.refs_0_, bf16[1024,1024]{1,0:T(8,128)(2,1)} %copy-done.1, bf16[1024,1024]{1,0:T(8,128)(2,1)} %copy-done.6, bf16[1024,1024]{1,0:T(8,128)(2,1)} %copy-done.5, bf16[1024,1024]{1,0:T(8,128)(2,1)} %copy-done.7, bf16[1040,1024]{1,0:T(8,128)(2,1)} %copy-done, ...), custom_call_target="tpu_custom_call" | custom-call | flops 5771362304 | bytes 23068672 | tf_op jit(solution)/shard_map/pallas_call | solution.py:50
  206.0 6.0 %convert_element_type.9 = f16[512,4224]{1,0:T(8,128)(2,1)} convert(f32[512,4224]{1,0:T(8,128)} %shard_map.85) | non-fusion elementwise | flops 2162688 | bytes 12976128 | tf_op jit(solution)/shard_map/convert_element_type | solution.py:348
  212.0 7.1 %all-to-all-start = ((f16[16,32,4224]{2,1,0:T(8,128)(2,1)}), f16[16,32,4224]{2,1,0:T(8,128)(2,1)}, u32[]{:S(2)}, u32[]{:S(2)}) async-start(f16[16,32,4224]{2,1,0:T(8,128)(2,1)} %bitcast.19), calls=%async_computation | async-start | bytes 8650752 | tf_op jit(solution)/shard_map/all_to_all | solution.py:349
  220.6 5.6 %collective-permute-start.25 = (bf16[4112,512]{1,0:T(8,128)(2,1)}, bf16[4112,512]{1,0:T(8,128)(2,1)}, u32[]{:S(2)}, u32[]{:S(2)}) collective-permute-start(bf16[4112,512]{1,0:T(8,128)(2,1)} %get-tuple-element.20), channel_id=1, source_target_pairs={{16,0},{17,1},{18,2},{19,3},{20,4},{21,5},{22,6},{23,7},{24,8},{25... | collective-permute-start | bytes 12632072 | tf_op jit(solution)/shard_map/ppermute | solution.py:37
  226.2 35.6 %collective-permute-done.13.refs_0_ = bf16[2064,512]{1,0:T(8,128)(2,1)} collective-permute-done((bf16[2064,512]{1,0:T(8,128)(2,1)S(1)}, bf16[2064,512]{1,0:T(8,128)(2,1)}, u32[]{:S(2)}, u32[]{:S(2)}) %collective-permute-start.13) | collective-permute-done | bytes 2113568 | tf_op jit(solution)/shard_map/ppermute | solution.py:37
  266.1 7.7 %collective-permute-start.24 = (bf16[2064,512]{1,0:T(8,128)(2,1)}, bf16[2064,512]{1,0:T(8,128)(2,1)}, u32[]{:S(2)}, u32[]{:S(2)}) collective-permute-start(bf16[2064,512]{1,0:T(8,128)(2,1)} %collective-permute-done.15.refs_3_), channel_id=1, source_target_pairs={{16,0},{17,1},{18,2},{19,3},{20,4},{21,5},{22,6},{23,7},{24,8},{25... | collective-permute-start | bytes 6340616 | tf_op jit(solution)/shard_map/ppermute | solution.py:37
  273.7 12.4 %collective-permute-done.16.refs_1_ = bf16[1024,512]{1,0:T(8,128)(2,1)S(1)} collective-permute-done((bf16[1024,512]{1,0:T(8,128)(2,1)S(1)}, bf16[1024,512]{1,0:T(8,128)(2,1)S(1)}, u32[]{:S(2)}, u32[]{:S(2)}) %collective-permute-start.16) | collective-permute-done | bytes 1048608 | tf_op jit(solution)/shard_map/ppermute | solution.py:37
  286.1 6.7 %collective-permute-start.22 = (bf16[1024,512]{1,0:T(8,128)(2,1)S(1)}, bf16[1024,512]{1,0:T(8,128)(2,1)}, u32[]{:S(2)}, u32[]{:S(2)}) collective-permute-start(bf16[1024,512]{1,0:T(8,128)(2,1)S(1)} %collective-permute-done.16.refs_1_), channel_id=1, source_target_pairs={{16,0},{17,1},{18,2},{19,3},{20,4},{21,5},{22,6},{23,7},{24,8},{25... | collective-permute-start | bytes 3145736 | tf_op jit(solution)/shard_map/ppermute | solution.py:37
  293.1 23.5 %copy.10 = f16[16,32,4224]{1,0,2:T(8,128)(2,1)} copy(f16[16,32,4224]{2,1,0:T(8,128)(2,1)} %all-to-all-done) | data formatting | bytes 8650752 | tf_op jit(solution)/shard_map/all_to_all | solution.py:349
  316.7 8.9 %convert_element_type.10 = f32[16,32,4224]{1,0,2:T(8,128)S(1)} convert(f16[16,32,4224]{1,0,2:T(8,128)(2,1)} %copy.10) | non-fusion elementwise | flops 2162688 | bytes 12976128 | tf_op jit(solution)/shard_map/convert_element_type | solution.py:350
  325.6 42.8 %fusion = bf16[32,4096]{0,1:T(8,128)(2,1)S(1)} fusion(f32[16,32,4224]{1,0,2:T(8,128)S(1)} %convert_element_type.10, f32[16,32]{1,0:T(8,128)S(1)} %fusion.3), kind=kLoop, calls=%fused_computation.1 | loop fusion | flops 4063232 | bytes 8652800 | tf_op jit(solution)/shard_map/reduce_sum | solution.py:352
  369.5 11.6 %shard_map.86 = (f32[688,1024]{1,0:T(8,128)}, f32[688,1024]{1,0:T(8,128)}, f32[688,1024]{1,0:T(8,128)}) custom-call(bf16[2064,512]{1,0:T(8,128)(2,1)} %get-tuple-element.17.refs_0_, bf16[512,1024]{1,0:T(8,128)(2,1)} %get-tuple-element.18.refs_1_, bf16[512,1024]{1,0:T(8,128)(2,1)} %get-tuple-element.19.refs_2_, bf16[4112,512]{1,0:T(8,128)(2,1)} %collective-permute-done.25.refs_3_), custom_call_target="tpu_custom_call" | custom-call | flops 4328521728 | bytes 25165824 | tf_op jit(solution)/shard_map/pallas_call | solution.py:50
  381.2 20.2 %shard_map.87 = (f32[688,1024]{1,0:T(8,128)}, f32[688,1024]{1,0:T(8,128)}, f32[688,1024]{1,0:T(8,128)}) custom-call(bf16[2064,512]{1,0:T(8,128)(2,1)} %collective-permute-done.13.refs_0_, bf16[16,12,32,1024]{3,2,1,0:T(8,128)(2,1)} %all-gather.5.cloned.1.call-done.refs_1_.refs_2_, bf16[2064,512]{1,0:T(8,128)(2,1)} %collective-permute-done.23.refs_2_, ...), custom_call_target="tpu_custom_call" | custom-call | flops 8657043456 | bytes 33554432 | tf_op jit(solution)/shard_map/pallas_call | solution.py:50
  402.4 13.0 %shard_map.88 = (f32[688,1024]{1,0:T(8,128)}, f32[688,1024]{1,0:T(8,128)}, f32[688,1024]{1,0:T(8,128)}) custom-call(bf16[1040,512]{1,0:T(8,128)(2,1)} %collective-permute-done.14.refs_0_, bf16[1024,512]{1,0:T(8,128)(2,1)} %copy-done.11, bf16[16,12,32,1024]{3,2,1,0:T(8,128)(2,1)} %all-gather.5.cloned.1.call-done.refs_1_.refs_2_, ...), custom_call_target="tpu_custom_call" | custom-call | flops 4328521728 | bytes 25165824 | tf_op jit(solution)/shard_map/pallas_call | solution.py:50
  (103 shorter events, 45.7 us)
Async XLA Ops:
  7.2 161.1 %all-gather.3.cloned.1.call-start = ((), (), s32[]{:S(2)}) async-start(), calls=%async_computation.1 | async-start | bytes 4456448 | tf_op jit(solution)/shard_map/all_gather | solution.py:321
  8.9 372.3 %all-gather.5.cloned.1.call-start = ((), (), s32[]{:S(2)}) async-start(), calls=%async_computation.2 | async-start | bytes 13369344 | tf_op jit(solution)/shard_map/all_gather | solution.py:331
  29.4 60.0 %collective-permute-start.8 = (bf16[1024,1024]{1,0:T(8,128)(2,1)S(1)}, bf16[1024,1024]{1,0:T(8,128)(2,1)S(1)}, u32[]{:S(2)}, u32[]{:S(2)}) collective-permute-start(bf16[1024,1024]{1,0:T(8,128)(2,1)S(1)} %pad_maximum_fusion.1.refs_6_.refs_1_), channel_id=1, source_target_pairs={{32,0},{33,1},{34,2},{35,3},{36,4},{37,5},{38,6},{39,7},{40,8},{41... | collective-permute-start | bytes 6291464 | tf_op jit(solution)/shard_map/ppermute | solution.py:37
  32.2 48.4 %collective-permute-start.11 = (bf16[1040,1024]{1,0:T(8,128)(2,1)S(1)}, bf16[1040,1024]{1,0:T(8,128)(2,1)S(1)}, u32[]{:S(2)}, u32[]{:S(2)}) collective-permute-start(bf16[1040,1024]{1,0:T(8,128)(2,1)S(1)} %pad_maximum_fusion.refs_10_.refs_5_), channel_id=1, source_target_pairs={{96,0},{97,1},{98,2},{99,3},{100,4},{101,5},{102,6},{103,7},{104,8... | collective-permute-start | bytes 6389768 | tf_op jit(solution)/shard_map/ppermute | solution.py:37
  34.6 13.9 %collective-permute-start.1 = (bf16[32,4096]{1,0:T(8,128)(2,1)S(1)}, bf16[32,4096]{1,0:T(8,128)(2,1)S(1)}, u32[]{:S(2)}, u32[]{:S(2)}) collective-permute-start(bf16[32,4096]{1,0:T(8,128)(2,1)S(1)} %pad_maximum_fusion.5), channel_id=1, source_target_pairs={{2,0},{3,1},{0,2},{1,3},{6,4},{7,5},{4,6},{5,7},{10,8},{11,9},{8,1... | collective-permute-start | bytes 786440 | tf_op jit(solution)/shard_map/ppermute | solution.py:37
  37.2 12.7 %collective-permute-start = (bf16[32,4096]{1,0:T(8,128)(2,1)S(1)}, bf16[32,4096]{1,0:T(8,128)(2,1)S(1)}, u32[]{:S(2)}, u32[]{:S(2)}) collective-permute-start(bf16[32,4096]{1,0:T(8,128)(2,1)S(1)} %pad_maximum_fusion.5), channel_id=1, source_target_pairs={{1,0},{2,1},{3,2},{0,3},{5,4},{6,5},{7,6},{4,7},{9,8},{10,9},{11,1... | collective-permute-start | bytes 786440 | tf_op jit(solution)/shard_map/ppermute | solution.py:37
  50.1 38.2 %collective-permute-start.4 = (bf16[128,4096]{1,0:T(8,128)(2,1)S(1)}, bf16[128,4096]{1,0:T(8,128)(2,1)S(1)}, u32[]{:S(2)}, u32[]{:S(2)}) collective-permute-start(bf16[128,4096]{1,0:T(8,128)(2,1)S(1)} %pad_maximum_fusion.2.refs_1_), channel_id=1, source_target_pairs={{12,0},{13,1},{14,2},{15,3},{0,4},{1,5},{2,6},{3,7},{4,8},{5,9},{6... | collective-permute-start | bytes 3145736 | tf_op jit(solution)/shard_map/ppermute | solution.py:37
  51.7 113.1 %collective-permute-start.10 = (bf16[1040,1024]{1,0:T(8,128)(2,1)S(1)}, bf16[1040,1024]{1,0:T(8,128)(2,1)S(1)}, u32[]{:S(2)}, u32[]{:S(2)}) collective-permute-start(bf16[1040,1024]{1,0:T(8,128)(2,1)S(1)} %pad_maximum_fusion.refs_10_.refs_5_), channel_id=1, source_target_pairs={{16,0},{17,1},{18,2},{19,3},{20,4},{21,5},{22,6},{23,7},{24,8},{25... | collective-permute-start | bytes 6389768 | tf_op jit(solution)/shard_map/ppermute | solution.py:37
  80.6 87.6 %collective-permute-start.12 = (bf16[1040,1024]{1,0:T(8,128)(2,1)S(1)}, bf16[1040,1024]{1,0:T(8,128)(2,1)}, u32[]{:S(2)}, u32[]{:S(2)}) collective-permute-start(bf16[1040,1024]{1,0:T(8,128)(2,1)S(1)} %collective-permute-done.11.refs_12_.refs_7_), channel_id=1, source_target_pairs={{16,0},{17,1},{18,2},{19,3},{20,4},{21,5},{22,6},{23,7},{24,8},{25... | collective-permute-start | bytes 6389768 | tf_op jit(solution)/shard_map/ppermute | solution.py:37
  82.3 39.0 %collective-permute-start.3 = (bf16[128,4096]{1,0:T(8,128)(2,1)S(1)}, bf16[128,4096]{1,0:T(8,128)(2,1)S(1)}, u32[]{:S(2)}, u32[]{:S(2)}) collective-permute-start(bf16[128,4096]{1,0:T(8,128)(2,1)S(1)} %pad_maximum_fusion.2.refs_1_), channel_id=1, source_target_pairs={{4,0},{5,1},{6,2},{7,3},{8,4},{9,5},{10,6},{11,7},{12,8},{13,9},{1... | collective-permute-start | bytes 3145736 | tf_op jit(solution)/shard_map/ppermute | solution.py:37
  88.3 76.5 %collective-permute-start.7 = (bf16[1024,1024]{1,0:T(8,128)(2,1)S(1)}, bf16[1024,1024]{1,0:T(8,128)(2,1)S(1)}, u32[]{:S(2)}, u32[]{:S(2)}) collective-permute-start(bf16[1024,1024]{1,0:T(8,128)(2,1)S(1)} %pad_maximum_fusion.1.refs_6_.refs_1_), channel_id=1, source_target_pairs={{16,0},{17,1},{18,2},{19,3},{20,4},{21,5},{22,6},{23,7},{24,8},{25... | collective-permute-start | bytes 6291464 | tf_op jit(solution)/shard_map/ppermute | solution.py:37
  89.4 75.4 %collective-permute-start.9 = (bf16[1024,1024]{1,0:T(8,128)(2,1)S(1)}, bf16[1024,1024]{1,0:T(8,128)(2,1)S(1)}, u32[]{:S(2)}, u32[]{:S(2)}) collective-permute-start(bf16[1024,1024]{1,0:T(8,128)(2,1)S(1)} %collective-permute-done.8.refs_8_.refs_3_), channel_id=1, source_target_pairs={{16,0},{17,1},{18,2},{19,3},{20,4},{21,5},{22,6},{23,7},{24,8},{25... | collective-permute-start | bytes 6291464 | tf_op jit(solution)/shard_map/ppermute | solution.py:37
  121.3 19.3 %collective-permute-start.6 = (bf16[64,4096]{1,0:T(8,128)(2,1)S(1)}, bf16[64,4096]{1,0:T(8,128)(2,1)S(1)}, u32[]{:S(2)}, u32[]{:S(2)}) collective-permute-start(bf16[64,4096]{1,0:T(8,128)(2,1)S(1)} %slice.97), channel_id=1, source_target_pairs={{12,0},{13,1},{14,2},{15,3},{0,4},{1,5},{2,6},{3,7},{4,8},{5,9},{6... | collective-permute-start | bytes 1572872 | tf_op jit(solution)/shard_map/ppermute | solution.py:37
  140.6 24.2 %collective-permute-start.5 = (bf16[64,4096]{1,0:T(8,128)(2,1)S(1)}, bf16[64,4096]{1,0:T(8,128)(2,1)S(1)}, u32[]{:S(2)}, u32[]{:S(2)}) collective-permute-start(bf16[64,4096]{1,0:T(8,128)(2,1)S(1)} %slice.96), channel_id=1, source_target_pairs={{4,0},{5,1},{6,2},{7,3},{8,4},{9,5},{10,6},{11,7},{12,8},{13,9},{1... | collective-permute-start | bytes 1572872 | tf_op jit(solution)/shard_map/ppermute | solution.py:37
  212.0 81.1 %all-to-all-start = ((f16[16,32,4224]{2,1,0:T(8,128)(2,1)}), f16[16,32,4224]{2,1,0:T(8,128)(2,1)}, u32[]{:S(2)}, u32[]{:S(2)}) async-start(f16[16,32,4224]{2,1,0:T(8,128)(2,1)} %bitcast.19), calls=%async_computation | async-start | bytes 8650752 | tf_op jit(solution)/shard_map/all_to_all | solution.py:349
  219.1 42.7 %collective-permute-start.13 = (bf16[2064,512]{1,0:T(8,128)(2,1)S(1)}, bf16[2064,512]{1,0:T(8,128)(2,1)}, u32[]{:S(2)}, u32[]{:S(2)}) collective-permute-start(bf16[2064,512]{1,0:T(8,128)(2,1)S(1)} %copy-done.4), channel_id=1, source_target_pairs={{32,0},{33,1},{34,2},{35,3},{36,4},{37,5},{38,6},{39,7},{40,8},{41... | collective-permute-start | bytes 6340616 | tf_op jit(solution)/shard_map/ppermute | solution.py:37
  219.2 45.5 %collective-permute-start.15 = (bf16[2064,512]{1,0:T(8,128)(2,1)S(1)}, bf16[2064,512]{1,0:T(8,128)(2,1)}, u32[]{:S(2)}, u32[]{:S(2)}) collective-permute-start(bf16[2064,512]{1,0:T(8,128)(2,1)S(1)} %copy-done.4), channel_id=1, source_target_pairs={{96,0},{97,1},{98,2},{99,3},{100,4},{101,5},{102,6},{103,7},{104,8... | collective-permute-start | bytes 6340616 | tf_op jit(solution)/shard_map/ppermute | solution.py:37
  220.6 148.9 %collective-permute-start.25 = (bf16[4112,512]{1,0:T(8,128)(2,1)}, bf16[4112,512]{1,0:T(8,128)(2,1)}, u32[]{:S(2)}, u32[]{:S(2)}) collective-permute-start(bf16[4112,512]{1,0:T(8,128)(2,1)} %get-tuple-element.20), channel_id=1, source_target_pairs={{16,0},{17,1},{18,2},{19,3},{20,4},{21,5},{22,6},{23,7},{24,8},{25... | collective-permute-start | bytes 12632072 | tf_op jit(solution)/shard_map/ppermute | solution.py:37
  263.1 29.7 %collective-permute-start.14 = (bf16[1040,512]{1,0:T(8,128)(2,1)S(1)}, bf16[1040,512]{1,0:T(8,128)(2,1)}, u32[]{:S(2)}, u32[]{:S(2)}) collective-permute-start(bf16[1040,512]{1,0:T(8,128)(2,1)S(1)} %slice.104), channel_id=1, source_target_pairs={{32,0},{33,1},{34,2},{35,3},{36,4},{37,5},{38,6},{39,7},{40,8},{41... | collective-permute-start | bytes 3194888 | tf_op jit(solution)/shard_map/ppermute | solution.py:37
  266.0 20.1 %collective-permute-start.16 = (bf16[1024,512]{1,0:T(8,128)(2,1)S(1)}, bf16[1024,512]{1,0:T(8,128)(2,1)S(1)}, u32[]{:S(2)}, u32[]{:S(2)}) collective-permute-start(bf16[1024,512]{1,0:T(8,128)(2,1)S(1)} %slice.105), channel_id=1, source_target_pairs={{96,0},{97,1},{98,2},{99,3},{100,4},{101,5},{102,6},{103,7},{104,8... | collective-permute-start | bytes 3145736 | tf_op jit(solution)/shard_map/ppermute | solution.py:37
  266.1 115.1 %collective-permute-start.24 = (bf16[2064,512]{1,0:T(8,128)(2,1)}, bf16[2064,512]{1,0:T(8,128)(2,1)}, u32[]{:S(2)}, u32[]{:S(2)}) collective-permute-start(bf16[2064,512]{1,0:T(8,128)(2,1)} %collective-permute-done.15.refs_3_), channel_id=1, source_target_pairs={{16,0},{17,1},{18,2},{19,3},{20,4},{21,5},{22,6},{23,7},{24,8},{25... | collective-permute-start | bytes 6340616 | tf_op jit(solution)/shard_map/ppermute | solution.py:37
  273.7 107.5 %collective-permute-start.23 = (bf16[2064,512]{1,0:T(8,128)(2,1)}, bf16[2064,512]{1,0:T(8,128)(2,1)}, u32[]{:S(2)}, u32[]{:S(2)}) collective-permute-start(bf16[2064,512]{1,0:T(8,128)(2,1)} %collective-permute-done.13.refs_0_), channel_id=1, source_target_pairs={{16,0},{17,1},{18,2},{19,3},{20,4},{21,5},{22,6},{23,7},{24,8},{25... | collective-permute-start | bytes 6340616 | tf_op jit(solution)/shard_map/ppermute | solution.py:37
  286.1 115.3 %collective-permute-start.22 = (bf16[1024,512]{1,0:T(8,128)(2,1)S(1)}, bf16[1024,512]{1,0:T(8,128)(2,1)}, u32[]{:S(2)}, u32[]{:S(2)}) collective-permute-start(bf16[1024,512]{1,0:T(8,128)(2,1)S(1)} %collective-permute-done.16.refs_1_), channel_id=1, source_target_pairs={{16,0},{17,1},{18,2},{19,3},{20,4},{21,5},{22,6},{23,7},{24,8},{25... | collective-permute-start | bytes 3145736 | tf_op jit(solution)/shard_map/ppermute | solution.py:37
  292.8 108.6 %collective-permute-start.21 = (bf16[1040,512]{1,0:T(8,128)(2,1)}, bf16[1040,512]{1,0:T(8,128)(2,1)S(1)}, u32[]{:S(2)}, u32[]{:S(2)}) collective-permute-start(bf16[1040,512]{1,0:T(8,128)(2,1)} %collective-permute-done.14.refs_0_), channel_id=1, source_target_pairs={{16,0},{17,1},{18,2},{19,3},{20,4},{21,5},{22,6},{23,7},{24,8},{25... | collective-permute-start | bytes 3194888 | tf_op jit(solution)/shard_map/ppermute | solution.py:37
  (24 other events, 649.1 us)
Sparse Core Ops, SparseCore 0:
  10.7 65.1 all-gather.2
  78.0 114.0 all-gather.4
where the time goes:
time: 423 us; the launch traced here: 422 us
  waiting for transfers between devices  172 us (41%)
  Pallas kernels  82.5 us (20%)
  other arithmetic  62.8 us (15%)
  starting transfers between devices  59.3 us (14%)
  local copies, waits for them, and re-layouts  31 us (7%)
  between operations  14.4 us (3%)
    ppermute x26, waiting for transfers between devices, moved(): return lax.ppermute(array, AXES, pairs)  172 us
    pallas_call x5, Pallas kernels, call(): pl.pallas_call(body, out_shape=out_shape, in_specs=ins, out_specs=outs, s...  82.5 us
    ppermute x26, starting transfers between devices, moved(): return lax.ppermute(array, AXES, pairs)  52.2 us
    reduce_sum x1, other arithmetic, block(): grad_inputs = jnp.sum(got[:, :, :WIDE] * back, axis=0).astype(BF)  42.8 us
    all_to_all x1, local copies, waits for them, and re-layouts, block(): got = lax.all_to_all(packed, 'tp', 0, 0, tiled=True)  23.5 us
    convert_element_type x1, other arithmetic, block(): got = got.reshape(16, ROWS, WIDE + TAIL).astype(F32)  8.95 us
  transfers between devices with their start and end apart: 29, of which 13 were waited for; matrix products, arithmetic and copies ran while one was open for 21% of the time, Pallas kernels for 16%

commit v1 on v0

v1 whole, which is shorter than its diff:
```python
import functools

import jax
import jax.numpy as jnp
from jax import lax
from jax.experimental import pallas as pl
from jax.experimental.pallas import tpu as pltpu
from jax.sharding import PartitionSpec as P


AXES = ("rep", "fs", "tp")
BF, F32, F16 = jnp.bfloat16, jnp.float32, jnp.float16
W_MAX = 0.09375
ANY = pl.BlockSpec(memory_space=pl.ANY)
VMEM = pl.BlockSpec(memory_space=pltpu.VMEM)
LIMIT = 56 * 1024 * 1024

ROWS, DEPTH, UNITS = 32, 1024, 688
TOK, WIDE = 16 * ROWS, 4 * DEPTH
CUT = 336
LOW = 1040
HALF = 2 * DEPTH
TAIL = 128


def index_of(x, c, z, y):
    x, z, y = x % 4, z % 4, y % 4
    return (x // 2) * 64 + ((x % 2) * 2 + c) * 16 + z * 4 + y


def moved(array, dx=0, flip=0, dz=0, dy=0):
    pairs = []
    for x in range(4):
        for c in range(2):
            for z in range(4):
                for y in range(4):
                    pairs.append((index_of(x + dx, c ^ flip, z + dz, y + dy), index_of(x, c, z, y)))
    return lax.ppermute(array, AXES, pairs)


def dot(a, b, ca, cb):
    return lax.dot_general(a, b, (((ca,), (cb,)), ((), ())), preferred_element_type=F32)


def place():
    tp = lax.axis_index("tp")
    return tp // 4, tp % 4


def call(body, out_shape, scratch, flops, ins, outs, args, nbytes):
    return pl.pallas_call(
        body,
        out_shape=out_shape,
        in_specs=ins,
        out_specs=outs,
        scratch_shapes=scratch,
        compiler_params=pltpu.CompilerParams(vmem_limit_bytes=LIMIT),
        cost_estimate=pl.CostEstimate(flops=flops, bytes_accessed=nbytes, transcendentals=0),
    )(*args)


FROM = ((0, 0, 4, 0), (1, 0, 4, 1), (2, 0, 4, 3), (3, 0, 2, 2), (4, 2, 2, 2))


def forward_kernel(*refs):
    xs, ds, was, wbs = refs[:5], refs[5:10], refs[10:14], refs[14:18]
    acts, side, x_own, d_own = refs[18:22]
    x, d, wa, wb, gate, up, back, act, sx, sd, sw, so = refs[22:]
    z, y = place()
    x_copies, d_copies = [], []
    for i, first, count, off in FROM:
        for j in range(count):
            row = pl.multiple_of((lax.rem(z + first + j, 4) * 4 + lax.rem(y + off, 4)) * ROWS, ROWS)
            x_copies.append(
                pltpu.make_async_copy(xs[i].at[pl.ds(j * ROWS, ROWS)], x.at[pl.ds(row, ROWS)], sx.at[len(x_copies)]))
            row = pl.multiple_of((lax.rem(z + off, 4) * 4 + lax.rem(y + first + j, 4)) * ROWS, ROWS)
            d_copies.append(
                pltpu.make_async_copy(ds[i].at[pl.ds(j * ROWS, ROWS)], d.at[pl.ds(row, ROWS)], sd.at[len(d_copies)]))
    w_copies = [
        [pltpu.make_async_copy(was[k], wa.at[k], sw.at[2 * k]), pltpu.make_async_copy(wbs[k], wb.at[k], sw.at[2 * k + 1])]
        for k in range(4)
    ]
    stages = [x_copies + w_copies[0], d_copies, w_copies[1], w_copies[2], w_copies[3]]

    def begin(n):
        if n < len(stages):
            for c in stages[n]:
                c.start()

    def end(n):
        for c in stages[n]:
            c.wait()

    def first(k):
        xk = x[:, k * DEPTH:(k + 1) * DEPTH]
        for into, w in ((gate, wa), (up, wb)):
            part = dot(w[k, :UNITS], xk, 1, 1)
            into[...] = part if k == 0 else into[...] + part

    def second(k):
        dk = d[:, k * DEPTH:(k + 1) * DEPTH]
        for rows, w in ((slice(0, CUT), wa), (slice(CUT, UNITS), wb)):
            part = dot(w[k, UNITS:], dk, 1, 1)
            back[rows, :] = part if k == 0 else back[rows, :] + part

    begin(0)
    begin(1)
    end(0)
    begin(2)
    first(0)
    end(1)
    begin(3)
    second(0)
    end(2)
    begin(4)
    outs = []
    for i, (v, to) in enumerate(((x, x_own), (d, d_own))):
        outs.append(pltpu.make_async_copy(v.at[:, pl.ds(0, DEPTH)], to, so.at[i]))
        for h in range(2):
            outs.append(pltpu.make_async_copy(
                v.at[:, pl.ds(DEPTH + h * TOK, TOK)],
                side.at[pl.ds(3 * UNITS + (2 * i + h) * TOK, TOK)], so.at[2 + 2 * i + h]))
    for k in (1, 2, 3):
        if k > 1:
            end(k + 1)
        if k == 3:
            for c in outs:
                c.start()
        first(k)
        second(k)

    def unit(i, _):
        r = pl.ds(pl.multiple_of(i * 16, 16), 16)
        g = gate[r, :].astype(BF).astype(F32)
        u = up[r, :].astype(BF).astype(F32)
        b = back[r, :].astype(BF).astype(F32)
        sigma = 1.0 / (1.0 + jnp.exp(-g))
        active = g * sigma
        act[r, :] = (b * u * sigma * (1.0 + g * (1.0 - sigma))).astype(BF)
        act[pl.ds(pl.multiple_of(UNITS + i * 16, 16), 16), :] = (b * active).astype(BF)
        act[pl.ds(pl.multiple_of(2 * UNITS + i * 16, 16), 16), :] = (active * u).astype(BF)
        return 0

    lax.fori_loop(0, UNITS // 16, unit, 0)
    outs.append(pltpu.make_async_copy(act, acts, so.at[6]))
    outs.append(pltpu.make_async_copy(act, side.at[pl.ds(0, 3 * UNITS)], so.at[7]))
    for c in outs[-2:]:
        c.start()
    for c in outs:
        c.wait()


def forward(xs, ds, was, wbs):
    shape = jax.ShapeDtypeStruct
    return call(
        forward_kernel,
        (shape((3 * UNITS, TOK), BF), shape((3 * UNITS + 4 * TOK, TOK), BF), shape((TOK, DEPTH), BF), shape((TOK, DEPTH), BF)),
        [
            pltpu.VMEM((TOK, WIDE), BF), pltpu.VMEM((TOK, WIDE), BF),
            pltpu.VMEM((4, UNITS + CUT, DEPTH), BF), pltpu.VMEM((4, 2 * UNITS - CUT, DEPTH), BF),
            pltpu.VMEM((UNITS, TOK), F32), pltpu.VMEM((UNITS, TOK), F32), pltpu.VMEM((UNITS, TOK), F32),
            pltpu.VMEM((3 * UNITS, TOK), BF),
            pltpu.SemaphoreType.DMA((16,)), pltpu.SemaphoreType.DMA((16,)),
            pltpu.SemaphoreType.DMA((8,)), pltpu.SemaphoreType.DMA((8,)),
        ],
        2 * TOK * WIDE * UNITS * 3,
        [ANY] * 18,
        (ANY,) * 4,
        (*xs, *ds, *was, *wbs),
        34 << 20,
    )


def input_kernel(*refs):
    acts, was, wbs = refs[0], refs[1:5], refs[5:9]
    own, away = refs[9:11], refs[11:13]
    wa, wb, tg, tu, total, expo, sw, so, st = refs[13:]
    z, y = place()
    copies = [
        (pltpu.make_async_copy(was[k].at[pl.ds(0, UNITS)], wa.at[k], sw.at[2 * k]),
         pltpu.make_async_copy(wbs[k].at[pl.ds(0, UNITS)], wb.at[k], sw.at[2 * k + 1]))
        for k in range(4)
    ]
    for pair in copies[:2]:
        for c in pair:
            c.start()
    tg[...] = acts[:UNITS, :].T
    tu[...] = acts[UNITS:2 * UNITS, :].T
    norm = jnp.sum(jnp.abs(tg[...].astype(F32)), axis=1, keepdims=True)
    norm = norm + jnp.sum(jnp.abs(tu[...].astype(F32)), axis=1, keepdims=True)
    e = jnp.ceil(jnp.log2(jnp.maximum(norm * (1.02 * W_MAX), 1e-30)))
    expo[...] = jnp.broadcast_to(e, (TOK, TAIL))

    def puts(src, side, cols, sems):
        out, n = [], 0
        for s in range(4):
            for i in range(4):
                zz, yy = (lax.rem(z + s, 4), i) if side == 0 else (i, lax.rem(y + s, 4))
                r = pl.ds(pl.multiple_of((zz * 4 + yy) * ROWS, ROWS), ROWS)
                to = own[side] if s == 0 else away[side].at[s - 1]
                out.append(pltpu.make_async_copy(src.at[r], to.at[pl.ds(i * ROWS, ROWS), cols], sems.at[n]))
                n += 1
        return out

    tails = [c for side in range(2) for c in puts(expo, side, pl.ds(HALF, TAIL), st.at[side])]
    for c in tails:
        c.start()
    pending = [None, None]
    for k in range(4):
        for c in copies[k]:
            c.wait()
        if k + 2 < 4:
            for c in copies[k + 2]:
                c.start()
        if pending[k % 2]:
            for c in pending[k % 2]:
                c.wait()
        v = dot(tg[...], wa[k], 1, 0) + dot(tu[...], wb[k], 1, 0)
        total[k % 2] = v * jnp.exp2(14.0 - expo[:, :1])
        pending[k % 2] = puts(total.at[k % 2], k // 2, pl.ds((k % 2) * DEPTH, DEPTH), so.at[k % 2])
        for c in pending[k % 2]:
            c.start()
    for c in pending[0] + pending[1] + tails:
        c.wait()


def input_sums(acts, was, wbs):
    shape = jax.ShapeDtypeStruct
    own, away = shape((4 * ROWS, HALF + TAIL), F32), shape((3, 4 * ROWS, HALF + TAIL), F32)
    return call(
        input_kernel,
        (own, own, away, away),
        [
            pltpu.VMEM((4, UNITS, DEPTH), BF), pltpu.VMEM((4, UNITS, DEPTH), BF),
            pltpu.VMEM((TOK, UNITS), BF), pltpu.VMEM((TOK, UNITS), BF),
            pltpu.VMEM((2, TOK, DEPTH), F32), pltpu.VMEM((TOK, TAIL), F32),
            pltpu.SemaphoreType.DMA((8,)), pltpu.SemaphoreType.DMA((2, 16)), pltpu.SemaphoreType.DMA((2, 16)),
        ],
        2 * TOK * WIDE * UNITS * 2,
        [VMEM] + [ANY] * 8,
        (ANY,) * 4,
        (acts, *was, *wbs),
        22 << 20,
    )


def join_kernel(*refs):
    z, y = place()
    for got, to, at in ((refs[0:4], refs[8], y), (refs[4:8], refs[9], z)):
        for s in range(4):
            r = pl.ds(pl.multiple_of(lax.rem(at + s, 4) * ROWS, ROWS), ROWS)
            v = None
            for g in got:
                w = g[r, :HALF] * jnp.exp2(g[r, HALF:HALF + 1] - 14.0)
                v = w if v is None else v + w
            to[s] = v


def joined(own_a, own_b, ra, rb):
    out = jax.ShapeDtypeStruct((4, ROWS, HALF), F32)
    return call(
        join_kernel, (out, out), [], 1 << 30, [VMEM] * 8, (VMEM,) * 2, (own_a, *ra, own_b, *rb), 12 << 20)


def weight_kernel(picks, has_base, n_in, *refs):
    ins, outs = refs[:n_in], refs[n_in:n_in + 3]
    a, xc, dc, total, sa, sc, sb, so = refs[n_in + 3:]
    stages = [[], [], []]
    n = 0
    for g, (pieces, x_at, d_at) in enumerate(picks):
        for i, r0, r1 in pieces:
            for s in range(3):
                lo, hi = max(r0, s * UNITS), min(r1, (s + 1) * UNITS)
                if lo < hi:
                    stages[s].append(pltpu.make_async_copy(
                        ins[i].at[pl.ds(lo - r0, hi - lo)], a.at[pl.ds(lo, hi - lo), pl.ds(g * TOK, TOK)], sa.at[n]))
                    n += 1
        for (i, sub), buf, s in ((x_at, xc, 0), (d_at, dc, 2)):
            if len(ins[i].shape) == 4:
                pairs = [(ins[i].at[:, sub], buf.at[g])]
            elif sub is None:
                pairs = [(ins[i], buf.at[g])]
            else:
                pairs = [(ins[i].at[pl.ds(sub + h * TOK, TOK)], buf.at[g, :, pl.ds(h * TOK, TOK)]) for h in range(2)]
            for h, (src, to) in enumerate(pairs):
                stages[s].append(pltpu.make_async_copy(src, to, sc.at[4 * g + s + h]))
    if has_base:
        for s in range(3):
            stages[s].append(pltpu.make_async_copy(ins[n_in - 3 + s], total.at[s], sb.at[s]))

    def begin(s):
        for c in stages[s]:
            c.start()

    begin(0)
    begin(1)
    done = []
    for i in range(3):
        for c in stages[i]:
            c.wait()
        if i == 0:
            begin(2)
        cols = dc if i == 2 else xc
        v = dot(a[i * UNITS:(i + 1) * UNITS, :], cols[...].reshape(len(picks) * TOK, DEPTH), 1, 0)
        total[i] = total[i] + v if has_base else v
        done.append(pltpu.make_async_copy(total.at[i], outs[i], so.at[i]))
        done[-1].start()
    for c in done:
        c.wait()


def weight_sums(groups, base):
    ins, picks = [], []

    def slot(v):
        for i, w in enumerate(ins):
            if w is v:
                return i
        ins.append(v)
        return len(ins) - 1

    n_pieces = 0
    tiled = groups[0][2][0].ndim == 4
    for pieces, rows, (xv, xi), (dv, di) in groups:
        row, marks = 0, []
        for p, m in zip(pieces, rows):
            marks.append((slot(p), row, row + m))
            row += m
            n_pieces += 1
        picks.append((marks, (slot(xv), xi), (slot(dv), di)))
    ins += list(base or [])
    n = len(groups)
    col = (n, 16, ROWS, DEPTH) if tiled else (n, TOK, DEPTH)
    out = jax.ShapeDtypeStruct((UNITS, DEPTH), F32)
    return call(
        functools.partial(weight_kernel, picks, base is not None, len(ins)),
        (out,) * 3,
        [
            pltpu.VMEM((3 * UNITS, n * TOK), BF), pltpu.VMEM(col, BF), pltpu.VMEM(col, BF),
            pltpu.VMEM((3, UNITS, DEPTH), F32),
            pltpu.SemaphoreType.DMA((3 * n_pieces,)), pltpu.SemaphoreType.DMA((4 * n,)),
            pltpu.SemaphoreType.DMA((3,)), pltpu.SemaphoreType.DMA((3,)),
        ],
        2 * 3 * UNITS * DEPTH * n * TOK,
        [ANY] * len(ins),
        (ANY,) * 3,
        ins,
        n * (4 << 20) + (16 << 20),
    )


def block(inputs, w_gate, w_up, w_down, d_out):
    fs = lax.axis_index("fs")

    def relative(v):
        parts = [v[:, i * DEPTH:(i + 1) * DEPTH] for i in range(4)]
        out = []
        for k in range(4):
            w = parts[k]
            for f in range(1, 4):
                w = jnp.where(fs == f, parts[f ^ k], w)
            out.append(w)
        return out

    xp, dp = relative(inputs), relative(d_out)
    x_own, d_own = jnp.concatenate(xp, axis=1), jnp.concatenate(dp, axis=1)

    def spread(own, first, second):
        line = jnp.concatenate([own] + [moved(own, **{first: d}) for d in (1, 2, 3)], axis=0)
        up, down = moved(line, **{second: 1}), moved(line, **{second: -1})
        h = 2 * ROWS
        return (line, up, down, moved(up[:h], **{second: 1}), moved(down[h:], **{second: -1}))

    xs = spread(x_own, "dz", "dy")
    ds = spread(d_own, "dy", "dz")

    side = moved(jnp.stack([xp[1], dp[1], xp[3], dp[3]]), flip=1)
    far = jnp.stack([xp[0], side[0], dp[0], side[1]])
    near = jnp.stack([xp[2], side[2], dp[2], side[3]])
    got = jnp.stack([moved(near, dx=1), moved(near, dx=-1), moved(far, dx=2)])
    cols = lax.all_gather(got.reshape(12, ROWS, DEPTH), "tp", axis=0)

    wa = jnp.concatenate([w_gate.T, w_down[:CUT]], axis=0)
    wb = jnp.concatenate([w_up.T, w_down[CUT:]], axis=0)
    wa2, wb2 = moved(wa, dx=1), moved(wb, dx=-1)
    wa1, wb1 = moved(wa, flip=1), moved(wb, flip=1)
    wa3, wb3 = moved(wa2, flip=1), moved(wb2, flip=1)
    was, wbs = (wa, wa1, wa2, wa3), (wb, wb1, wb2, wb3)

    acts, side, x_cols, d_cols = forward(xs, ds, was, wbs)

    am, ap = moved(acts, dx=1), moved(acts, dx=-1)
    side = moved(side, flip=1)
    oa, ob = moved(am[:LOW], dx=1), moved(ap[LOW:], dx=-1)
    sm, sp = moved(am, flip=1), moved(ap, flip=1)
    soa, sob = moved(oa, flip=1), moved(ob, flip=1)

    own_a, own_b, qa, qb = input_sums(acts, was, wbs)
    qa, qb = qa.astype(F16), qb.astype(F16)
    ra = [moved(qa[d - 1], dz=-d).astype(F32) for d in (1, 2, 3)]
    rb = [moved(qb[d - 1], dy=-d).astype(F32) for d in (1, 2, 3)]
    fa, fb = joined(own_a, own_b, ra, rb)
    fa = fa[0] + moved(fa[1], dy=-1) + moved(fa[2], dy=-2) + moved(fa[3], dy=-3)
    fb = fb[0] + moved(fb[1], dz=-1) + moved(fb[2], dz=-2) + moved(fb[3], dz=-3)
    grad_inputs = jnp.concatenate(relative(jnp.concatenate([fa, fb], axis=1).astype(BF)), axis=1)

    full, cut = (3 * UNITS,), (LOW, 3 * UNITS - LOW)
    at = 3 * UNITS
    sums = weight_sums(
        [([acts], full, (x_cols, None), (d_cols, None)), ([side], full, (side, at), (side, at + 2 * TOK))], None)
    sums = weight_sums(
        [([am], full, (cols, 0), (cols, 2)), ([sm], full, (cols, 1), (cols, 3)),
         ([ap], full, (cols, 4), (cols, 6)), ([sp], full, (cols, 5), (cols, 7))], sums)
    sums = weight_sums(
        [([oa, ob], cut, (cols, 8), (cols, 10)), ([soa, sob], cut, (cols, 9), (cols, 11))], sums)
    return grad_inputs, sums[0].T, sums[1].T, sums[2]


def solution(mesh):
    tok = P(AXES, None)
    return jax.shard_map(
        block,
        mesh=mesh,
        in_specs=(tok, P("fs", "tp"), P("fs", "tp"), P("tp", "fs"), tok),
        out_specs=(tok, P("fs", "tp"), P("fs", "tp"), P("tp", "fs")),
        check_vma=False,
    )
```

time: 423 us -> 408 us (0.965); the launches traced: 422 us -> 400 us
  other arithmetic: 62.8 us -> 14.5 us
  starting transfers between devices: 59.3 us -> 102 us
  local copies, waits for them, and re-layouts: 31 us -> 6.52 us
  waiting for transfers between devices: 172 us -> 192 us
  Pallas kernels: 82.5 us -> 71 us
    ppermute x26 -> x45, starting transfers between devices: 52.2 us -> 102 us  [moved(): return lax.ppermute(array, AXES, pairs)]
    reduce_sum x1 -> x0, other arithmetic: 42.8 us -> none  [block(): grad_inputs = jnp.sum(got[:, :, :WIDE] * back, axis=0).astype(BF)]
    all_to_all x1 -> x0, local copies, waits for them, and re-layouts: 23.5 us -> none  [block(): got = lax.all_to_all(packed, 'tp', 0, 0, tiled=True)]
    ppermute x26 -> x45, waiting for transfers between devices: 172 us -> 192 us  [moved(): return lax.ppermute(array, AXES, pairs)]
    pallas_call x5 -> x6, Pallas kernels: 82.5 us -> 71 us  [call(): pl.pallas_call(body, out_shape=out_shape, in_specs=ins, out_specs=outs, s...]
    all_to_all x1 -> x0, starting transfers between devices: 7.08 us -> none  [block(): got = lax.all_to_all(packed, 'tp', 0, 0, tiled=True)]
    convert_element_type x2 -> x8, other arithmetic: 15 us -> 8.81 us  [the longest x3 3.32 us: block(): rb = [moved(qb[d - 1], dy=-d).astype(F32) for d in (1, 2, 3)]]
  transfers between devices with their start and end apart: 29 -> 46, of which waited for: 13 -> 25; matrix products, arithmetic and copies ran while one was open for 21% -> 3% of each run, Pallas kernels for 16% -> 15%
where the time goes in v1:
time: 408 us; the launch traced here: 400 us
  waiting for transfers between devices  192 us (47%)
  starting transfers between devices  102 us (25%)
  Pallas kernels  71 us (17%)
  between operations  14.8 us (4%)
  other arithmetic  14.5 us (4%)
  local copies, waits for them, and re-layouts  6.52 us (2%)
    ppermute x45, waiting for transfers between devices, moved(): return lax.ppermute(array, AXES, pairs)  192 us
    ppermute x45, starting transfers between devices, moved(): return lax.ppermute(array, AXES, pairs)  102 us
    pallas_call x6, Pallas kernels, call(): pl.pallas_call(body, out_shape=out_shape, in_specs=ins, out_specs=outs, s...  71 us
  transfers between devices with their start and end apart: 46, of which 25 were waited for; matrix products, arithmetic and copies ran while one was open for 3% of the time, Pallas kernels for 15%

profile of v1, /device:TPU:1, one launch (start us, length us, event | category | flops | bytes accessed | tf_op | source)
XLA Modules:
  0.0 400.2 jit_solution(10031988578543266312)
XLA Ops:
  21.0 6.3 %collective-permute-done.38 = bf16[4,32,1024]{2,1,0:T(8,128)(2,1)S(1)} collective-permute-done((bf16[4,32,1024]{2,1,0:T(8,128)(2,1)S(1)}, bf16[4,32,1024]{2,1,0:T(8,128)(2,1)S(1)}, u32[]{:S(2)}, u32[]{:S(2)}) %collective-permute-start.38) | collective-permute-done | bytes 262176 | tf_op jit(solution)/shard_map/ppermute | solution.py:38
  38.4 6.5 %collective-permute-done.1 = bf16[32,4096]{1,0:T(8,128)(2,1)S(1)} collective-permute-done((bf16[32,4096]{1,0:T(8,128)(2,1)S(1)}, bf16[32,4096]{1,0:T(8,128)(2,1)S(1)}, u32[]{:S(2)}, u32[]{:S(2)}) %collective-permute-start.1) | collective-permute-done | bytes 262176 | tf_op jit(solution)/shard_map/ppermute | solution.py:38
  51.1 12.7 %collective-permute-done.9 = bf16[32,4096]{1,0:T(8,128)(2,1)S(1)} collective-permute-done((bf16[32,4096]{1,0:T(8,128)(2,1)S(1)}, bf16[32,4096]{1,0:T(8,128)(2,1)S(1)}, u32[]{:S(2)}, u32[]{:S(2)}) %collective-permute-start.9) | collective-permute-done | bytes 262176 | tf_op jit(solution)/shard_map/ppermute | solution.py:38
  63.9 5.4 %collective-permute-done.8 = bf16[32,4096]{1,0:T(8,128)(2,1)S(1)} collective-permute-done((bf16[32,4096]{1,0:T(8,128)(2,1)S(1)}, bf16[32,4096]{1,0:T(8,128)(2,1)S(1)}, u32[]{:S(2)}, u32[]{:S(2)}) %collective-permute-start.8) | collective-permute-done | bytes 262176 | tf_op jit(solution)/shard_map/ppermute | solution.py:38
  69.3 22.6 %collective-permute-start.4 = (bf16[128,4096]{1,0:T(8,128)(2,1)S(1)}, bf16[128,4096]{1,0:T(8,128)(2,1)S(1)}, u32[]{:S(2)}, u32[]{:S(2)}) collective-permute-start(bf16[128,4096]{1,0:T(8,128)(2,1)S(1)} %pad_maximum_fusion.2.refs_0_), channel_id=1, source_target_pairs={{3,0},{0,1},{1,2},{2,3},{7,4},{4,5},{5,6},{6,7},{11,8},{8,9},{9,10... | collective-permute-start | bytes 3145736 | tf_op jit(solution)/shard_map/ppermute | solution.py:38
  91.9 8.1 %collective-permute-done.7 = bf16[32,4096]{1,0:T(8,128)(2,1)S(1)} collective-permute-done((bf16[32,4096]{1,0:T(8,128)(2,1)S(1)}, bf16[32,4096]{1,0:T(8,128)(2,1)S(1)}, u32[]{:S(2)}, u32[]{:S(2)}) %collective-permute-start.7) | collective-permute-done | bytes 262176 | tf_op jit(solution)/shard_map/ppermute | solution.py:38
  104.0 32.0 %collective-permute-done.4.refs_2_ = bf16[128,4096]{1,0:T(8,128)(2,1)S(1)} collective-permute-done((bf16[128,4096]{1,0:T(8,128)(2,1)S(1)}, bf16[128,4096]{1,0:T(8,128)(2,1)S(1)}, u32[]{:S(2)}, u32[]{:S(2)}) %collective-permute-start.4) | collective-permute-done | bytes 1048608 | tf_op jit(solution)/shard_map/ppermute | solution.py:38
  141.2 7.5 %collective-permute-done.10.refs_6_ = bf16[128,4096]{1,0:T(8,128)(2,1)S(1)} collective-permute-done((bf16[128,4096]{1,0:T(8,128)(2,1)S(1)}, bf16[128,4096]{1,0:T(8,128)(2,1)S(1)}, u32[]{:S(2)}, u32[]{:S(2)}) %collective-permute-start.10) | collective-permute-done | bytes 1048608 | tf_op jit(solution)/shard_map/ppermute | solution.py:38
  153.6 6.2 %collective-permute-done.5.refs_3_ = bf16[64,4096]{1,0:T(8,128)(2,1)S(1)} collective-permute-done((bf16[64,4096]{1,0:T(8,128)(2,1)S(1)}, bf16[64,4096]{1,0:T(8,128)(2,1)S(1)}, u32[]{:S(2)}, u32[]{:S(2)}) %collective-permute-start.5) | collective-permute-done | bytes 524320 | tf_op jit(solution)/shard_map/ppermute | solution.py:38
  160.1 11.1 %collective-permute-done.6.refs_4_ = bf16[64,4096]{1,0:T(8,128)(2,1)S(1)} collective-permute-done((bf16[64,4096]{1,0:T(8,128)(2,1)S(1)}, bf16[64,4096]{1,0:T(8,128)(2,1)S(1)}, u32[]{:S(2)}, u32[]{:S(2)}) %collective-permute-start.6) | collective-permute-done | bytes 524320 | tf_op jit(solution)/shard_map/ppermute | solution.py:38
  171.2 6.2 %collective-permute-start.12 = (bf16[64,4096]{1,0:T(8,128)(2,1)S(1)}, bf16[64,4096]{1,0:T(8,128)(2,1)S(1)}, u32[]{:S(2)}, u32[]{:S(2)}) collective-permute-start(bf16[64,4096]{1,0:T(8,128)(2,1)S(1)} %slice.158), channel_id=1, source_target_pairs={{4,0},{5,1},{6,2},{7,3},{8,4},{9,5},{10,6},{11,7},{12,8},{13,9},{1... | collective-permute-start | bytes 1572872 | tf_op jit(solution)/shard_map/ppermute | solution.py:38
  177.5 8.4 %collective-permute-done.12.refs_8_ = bf16[64,4096]{1,0:T(8,128)(2,1)S(1)} collective-permute-done((bf16[64,4096]{1,0:T(8,128)(2,1)S(1)}, bf16[64,4096]{1,0:T(8,128)(2,1)S(1)}, u32[]{:S(2)}, u32[]{:S(2)}) %collective-permute-start.12) | collective-permute-done | bytes 524320 | tf_op jit(solution)/shard_map/ppermute | solution.py:38
  186.4 12.1 %collective-permute-done.13.refs_9_ = bf16[64,4096]{1,0:T(8,128)(2,1)S(1)} collective-permute-done((bf16[64,4096]{1,0:T(8,128)(2,1)S(1)}, bf16[64,4096]{1,0:T(8,128)(2,1)S(1)}, u32[]{:S(2)}, u32[]{:S(2)}) %collective-permute-start.13) | collective-permute-done | bytes 524320 | tf_op jit(solution)/shard_map/ppermute | solution.py:38
  201.8 18.6 %shard_map.84 = (bf16[2064,512]{1,0:T(8,128)(2,1)}, bf16[4112,512]{1,0:T(8,128)(2,1)}, bf16[512,1024]{1,0:T(8,128)(2,1)}, bf16[512,1024]{1,0:T(8,128)(2,1)}) custom-call(bf16[128,4096]{1,0:T(8,128)(2,1)} %copy-done.8, bf16[128,4096]{1,0:T(8,128)(2,1)} %copy-done.13, bf16[128,4096]{1,0:T(8,128)(2,1)} %copy-done.14, bf16[64,4096]{1,0:T(8,128)(2,1)} %copy-done.22, ...), custom_call_target="tpu_custom_call" | custom-call | flops 8657043456 | bytes 35651584 | tf_op jit(solution)/shard_map/pallas_call | solution.py:51
  220.4 12.9 %shard_map.85 = (f32[128,2176]{1,0:T(8,128)}, f32[128,2176]{1,0:T(8,128)}, f32[3,128,2176]{2,1,0:T(8,128)}, f32[3,128,2176]{2,1,0:T(8,128)}) custom-call(bf16[2064,512]{1,0:T(8,128)(2,1)} %get-tuple-element.23.refs_0_, bf16[1024,1024]{1,0:T(8,128)(2,1)} %copy-done.2, bf16[1024,1024]{1,0:T(8,128)(2,1)} %copy-done.20, bf16[1024,1024]{1,0:T(8,128)(2,1)} %copy-done.19, ...), custom_call_target="tpu_custom_call" | custom-call | flops 5771362304 | bytes 23068672 | tf_op jit(solution)/shard_map/pallas_call | solution.py:51
  250.1 8.3 %collective-permute-done.21 = f16[128,2176]{1,0:T(8,128)(2,1)S(1)} collective-permute-done((f16[128,2176]{1,0:T(8,128)(2,1)S(1)}, f16[128,2176]{1,0:T(8,128)(2,1)S(1)}, u32[]{:S(2)}, u32[]{:S(2)}) %collective-permute-start.21) | collective-permute-done | bytes 557088 | tf_op jit(solution)/shard_map/ppermute | solution.py:38
  274.9 9.8 %collective-permute-done.25 = f16[128,2176]{1,0:T(8,128)(2,1)S(1)} collective-permute-done((f16[128,2176]{1,0:T(8,128)(2,1)S(1)}, f16[128,2176]{1,0:T(8,128)(2,1)S(1)}, u32[]{:S(2)}, u32[]{:S(2)}) %collective-permute-start.25) | collective-permute-done | bytes 557088 | tf_op jit(solution)/shard_map/ppermute | solution.py:38
  285.8 5.3 %shard_map.86 = (f32[4,32,2048]{2,1,0:T(8,128)}, f32[4,32,2048]{2,1,0:T(8,128)}) custom-call(f32[128,2176]{1,0:T(8,128)} %get-tuple-element.24.refs_0_, f32[128,2176]{1,0:T(8,128)} %convert_element_type.26.refs_1_, f32[128,2176]{1,0:T(8,128)} %convert_element_type.27.refs_2_, f32[128,2176]{1,0:T(8,128)} %convert_element_type.28.refs_3_, ...), custom_call_target="tpu_custom_call" | custom-call | flops 1073741824 | bytes 12582912 | tf_op jit(solution)/shard_map/pallas_call | solution.py:51
  310.5 5.5 %collective-permute-start.42 = (bf16[2064,512]{1,0:T(8,128)(2,1)S(1)}, bf16[2064,512]{1,0:T(8,128)(2,1)}, u32[]{:S(2)}, u32[]{:S(2)}) collective-permute-start(bf16[2064,512]{1,0:T(8,128)(2,1)S(1)} %collective-permute-done.32.refs_0_), channel_id=1, source_target_pairs={{16,0},{17,1},{18,2},{19,3},{20,4},{21,5},{22,6},{23,7},{24,8},{25... | collective-permute-start | bytes 6340616 | tf_op jit(solution)/shard_map/ppermute | solution.py:38
  317.9 7.2 %collective-permute-done.27 = f32[32,2048]{1,0:T(8,128)S(1)} collective-permute-done((f32[32,2048]{1,0:T(8,128)S(1)}, f32[32,2048]{1,0:T(8,128)S(1)}, u32[]{:S(2)}, u32[]{:S(2)}) %collective-permute-start.27) | collective-permute-done | bytes 262176 | tf_op jit(solution)/shard_map/ppermute | solution.py:38
  330.8 22.8 %collective-permute-done.35.refs_1_ = bf16[1024,512]{1,0:T(8,128)(2,1)S(1)} collective-permute-done((bf16[1024,512]{1,0:T(8,128)(2,1)S(1)}, bf16[1024,512]{1,0:T(8,128)(2,1)S(1)}, u32[]{:S(2)}, u32[]{:S(2)}) %collective-permute-start.35) | collective-permute-done | bytes 1048608 | tf_op jit(solution)/shard_map/ppermute | solution.py:38
  357.7 8.8 %shard_map.87 = (f32[688,1024]{1,0:T(8,128)}, f32[688,1024]{1,0:T(8,128)}, f32[688,1024]{1,0:T(8,128)}) custom-call(bf16[2064,512]{1,0:T(8,128)(2,1)} %get-tuple-element.23.refs_0_, bf16[512,1024]{1,0:T(8,128)(2,1)} %get-tuple-element.30.refs_1_, bf16[512,1024]{1,0:T(8,128)(2,1)} %get-tuple-element.31.refs_2_, bf16[4112,512]{1,0:T(8,128)(2,1)} %collective-permute-done.44.refs_3_), custom_call_target="tpu_custom_call" | custom-call | flops 4328521728 | bytes 25165824 | tf_op jit(solution)/shard_map/pallas_call | solution.py:51
  366.6 15.6 %shard_map.88 = (f32[688,1024]{1,0:T(8,128)}, f32[688,1024]{1,0:T(8,128)}, f32[688,1024]{1,0:T(8,128)}) custom-call(bf16[2064,512]{1,0:T(8,128)(2,1)} %copy-done.11, bf16[16,12,32,1024]{3,2,1,0:T(8,128)(2,1)} %all-gather.2.cloned.1.call-done.refs_1_.refs_2_, bf16[2064,512]{1,0:T(8,128)(2,1)} %collective-permute-done.42.refs_2_, ...), custom_call_target="tpu_custom_call" | custom-call | flops 8657043456 | bytes 33554432 | tf_op jit(solution)/shard_map/pallas_call | solution.py:51
  383.2 9.9 %shard_map.89 = (f32[688,1024]{1,0:T(8,128)}, f32[688,1024]{1,0:T(8,128)}, f32[688,1024]{1,0:T(8,128)}) custom-call(bf16[1040,512]{1,0:T(8,128)(2,1)} %copy-done.5, bf16[1024,512]{1,0:T(8,128)(2,1)} %copy-done.7, bf16[16,12,32,1024]{3,2,1,0:T(8,128)(2,1)} %all-gather.2.cloned.1.call-done.refs_1_.refs_2_, bf16[1040,512]{1,0:T(8,128)(2,1)} %copy-done.6, ...), custom_call_target="tpu_custom_call" | custom-call | flops 4328521728 | bytes 25165824 | tf_op jit(solution)/shard_map/pallas_call | solution.py:51
  (166 shorter events, 115.6 us)
Async XLA Ops:
  7.2 359.5 %all-gather.2.cloned.1.call-start = ((), (), s32[]{:S(2)}) async-start(), calls=%async_computation | async-start | bytes 13369344 | tf_op jit(solution)/shard_map/all_gather | solution.py:381
  34.4 119.0 %collective-permute-start.15 = (bf16[1024,1024]{1,0:T(8,128)(2,1)S(1)}, bf16[1024,1024]{1,0:T(8,128)(2,1)S(1)}, u32[]{:S(2)}, u32[]{:S(2)}) collective-permute-start(bf16[1024,1024]{1,0:T(8,128)(2,1)S(1)} %pad_maximum_fusion.1.refs_10_.refs_1_), channel_id=1, source_target_pairs={{32,0},{33,1},{34,2},{35,3},{36,4},{37,5},{38,6},{39,7},{40,8},{41... | collective-permute-start | bytes 6291464 | tf_op jit(solution)/shard_map/ppermute | solution.py:38
  37.2 103.9 %collective-permute-start.18 = (bf16[1040,1024]{1,0:T(8,128)(2,1)S(1)}, bf16[1040,1024]{1,0:T(8,128)(2,1)S(1)}, u32[]{:S(2)}, u32[]{:S(2)}) collective-permute-start(bf16[1040,1024]{1,0:T(8,128)(2,1)S(1)} %pad_maximum_fusion.refs_14_.refs_5_), channel_id=1, source_target_pairs={{96,0},{97,1},{98,2},{99,3},{100,4},{101,5},{102,6},{103,7},{104,8... | collective-permute-start | bytes 6389768 | tf_op jit(solution)/shard_map/ppermute | solution.py:38
  46.6 57.4 %collective-permute-start.3 = (bf16[128,4096]{1,0:T(8,128)(2,1)S(1)}, bf16[128,4096]{1,0:T(8,128)(2,1)S(1)}, u32[]{:S(2)}, u32[]{:S(2)}) collective-permute-start(bf16[128,4096]{1,0:T(8,128)(2,1)S(1)} %pad_maximum_fusion.2.refs_0_), channel_id=1, source_target_pairs={{1,0},{2,1},{3,2},{0,3},{5,4},{6,5},{7,6},{4,7},{9,8},{10,9},{11,1... | collective-permute-start | bytes 3145736 | tf_op jit(solution)/shard_map/ppermute | solution.py:38
  63.9 36.2 %collective-permute-start.7 = (bf16[32,4096]{1,0:T(8,128)(2,1)S(1)}, bf16[32,4096]{1,0:T(8,128)(2,1)S(1)}, u32[]{:S(2)}, u32[]{:S(2)}) collective-permute-start(bf16[32,4096]{1,0:T(8,128)(2,1)S(1)} %pad_maximum_fusion.6), channel_id=1, source_target_pairs={{1,0},{2,1},{3,2},{0,3},{5,4},{6,5},{7,6},{4,7},{9,8},{10,9},{11,1... | collective-permute-start | bytes 786440 | tf_op jit(solution)/shard_map/ppermute | solution.py:38
  69.3 66.7 %collective-permute-start.4 = (bf16[128,4096]{1,0:T(8,128)(2,1)S(1)}, bf16[128,4096]{1,0:T(8,128)(2,1)S(1)}, u32[]{:S(2)}, u32[]{:S(2)}) collective-permute-start(bf16[128,4096]{1,0:T(8,128)(2,1)S(1)} %pad_maximum_fusion.2.refs_0_), channel_id=1, source_target_pairs={{3,0},{0,1},{1,2},{2,3},{7,4},{4,5},{5,6},{6,7},{11,8},{8,9},{9,10... | collective-permute-start | bytes 3145736 | tf_op jit(solution)/shard_map/ppermute | solution.py:38
  100.2 48.5 %collective-permute-start.10 = (bf16[128,4096]{1,0:T(8,128)(2,1)S(1)}, bf16[128,4096]{1,0:T(8,128)(2,1)S(1)}, u32[]{:S(2)}, u32[]{:S(2)}) collective-permute-start(bf16[128,4096]{1,0:T(8,128)(2,1)S(1)} %pad_maximum_fusion.3.refs_5_), channel_id=1, source_target_pairs={{4,0},{5,1},{6,2},{7,3},{8,4},{9,5},{10,6},{11,7},{12,8},{13,9},{1... | collective-permute-start | bytes 3145736 | tf_op jit(solution)/shard_map/ppermute | solution.py:38
  103.9 48.3 %collective-permute-start.11 = (bf16[128,4096]{1,0:T(8,128)(2,1)S(1)}, bf16[128,4096]{1,0:T(8,128)(2,1)S(1)}, u32[]{:S(2)}, u32[]{:S(2)}) collective-permute-start(bf16[128,4096]{1,0:T(8,128)(2,1)S(1)} %pad_maximum_fusion.3.refs_5_), channel_id=1, source_target_pairs={{12,0},{13,1},{14,2},{15,3},{0,4},{1,5},{2,6},{3,7},{4,8},{5,9},{6... | collective-permute-start | bytes 3145736 | tf_op jit(solution)/shard_map/ppermute | solution.py:38
  136.0 62.4 %collective-permute-start.17 = (bf16[1040,1024]{1,0:T(8,128)(2,1)S(1)}, bf16[1040,1024]{1,0:T(8,128)(2,1)S(1)}, u32[]{:S(2)}, u32[]{:S(2)}) collective-permute-start(bf16[1040,1024]{1,0:T(8,128)(2,1)S(1)} %pad_maximum_fusion.refs_14_.refs_5_), channel_id=1, source_target_pairs={{16,0},{17,1},{18,2},{19,3},{20,4},{21,5},{22,6},{23,7},{24,8},{25... | collective-permute-start | bytes 6389768 | tf_op jit(solution)/shard_map/ppermute | solution.py:38
  141.1 60.7 %collective-permute-start.19 = (bf16[1040,1024]{1,0:T(8,128)(2,1)S(1)}, bf16[1040,1024]{1,0:T(8,128)(2,1)}, u32[]{:S(2)}, u32[]{:S(2)}) collective-permute-start(bf16[1040,1024]{1,0:T(8,128)(2,1)S(1)} %collective-permute-done.18.refs_16_.refs_7_), channel_id=1, source_target_pairs={{16,0},{17,1},{18,2},{19,3},{20,4},{21,5},{22,6},{23,7},{24,8},{25... | collective-permute-start | bytes 6389768 | tf_op jit(solution)/shard_map/ppermute | solution.py:38
  152.3 46.2 %collective-permute-start.14 = (bf16[1024,1024]{1,0:T(8,128)(2,1)S(1)}, bf16[1024,1024]{1,0:T(8,128)(2,1)S(1)}, u32[]{:S(2)}, u32[]{:S(2)}) collective-permute-start(bf16[1024,1024]{1,0:T(8,128)(2,1)S(1)} %pad_maximum_fusion.1.refs_10_.refs_1_), channel_id=1, source_target_pairs={{16,0},{17,1},{18,2},{19,3},{20,4},{21,5},{22,6},{23,7},{24,8},{25... | collective-permute-start | bytes 6291464 | tf_op jit(solution)/shard_map/ppermute | solution.py:38
  153.5 45.0 %collective-permute-start.16 = (bf16[1024,1024]{1,0:T(8,128)(2,1)S(1)}, bf16[1024,1024]{1,0:T(8,128)(2,1)S(1)}, u32[]{:S(2)}, u32[]{:S(2)}) collective-permute-start(bf16[1024,1024]{1,0:T(8,128)(2,1)S(1)} %collective-permute-done.15.refs_12_.refs_3_), channel_id=1, source_target_pairs={{16,0},{17,1},{18,2},{19,3},{20,4},{21,5},{22,6},{23,7},{24,8},{25... | collective-permute-start | bytes 6291464 | tf_op jit(solution)/shard_map/ppermute | solution.py:38
  235.8 22.6 %collective-permute-start.21 = (f16[128,2176]{1,0:T(8,128)(2,1)S(1)}, f16[128,2176]{1,0:T(8,128)(2,1)S(1)}, u32[]{:S(2)}, u32[]{:S(2)}) collective-permute-start(f16[128,2176]{1,0:T(8,128)(2,1)S(1)} %get-tuple-element.46), channel_id=1, source_target_pairs={{8,0},{9,1},{10,2},{11,3},{12,4},{13,5},{14,6},{15,7},{0,8},{1,9},... | collective-permute-start | bytes 1671176 | tf_op jit(solution)/shard_map/ppermute | solution.py:38
  238.2 24.3 %collective-permute-start.22 = (f16[128,2176]{1,0:T(8,128)(2,1)S(1)}, f16[128,2176]{1,0:T(8,128)(2,1)S(1)}, u32[]{:S(2)}, u32[]{:S(2)}) collective-permute-start(f16[128,2176]{1,0:T(8,128)(2,1)S(1)} %get-tuple-element.45), channel_id=1, source_target_pairs={{4,0},{5,1},{6,2},{7,3},{8,4},{9,5},{10,6},{11,7},{12,8},{13,9},{1... | collective-permute-start | bytes 1671176 | tf_op jit(solution)/shard_map/ppermute | solution.py:38
  238.7 119.0 %collective-permute-start.44 = (bf16[4112,512]{1,0:T(8,128)(2,1)}, bf16[4112,512]{1,0:T(8,128)(2,1)}, u32[]{:S(2)}, u32[]{:S(2)}) collective-permute-start(bf16[4112,512]{1,0:T(8,128)(2,1)} %get-tuple-element.32), channel_id=1, source_target_pairs={{16,0},{17,1},{18,2},{19,3},{20,4},{21,5},{22,6},{23,7},{24,8},{25... | collective-permute-start | bytes 12632072 | tf_op jit(solution)/shard_map/ppermute | solution.py:38
  247.6 62.9 %collective-permute-start.32 = (bf16[2064,512]{1,0:T(8,128)(2,1)}, bf16[2064,512]{1,0:T(8,128)(2,1)S(1)}, u32[]{:S(2)}, u32[]{:S(2)}) collective-permute-start(bf16[2064,512]{1,0:T(8,128)(2,1)} %get-tuple-element.23.refs_0_), channel_id=1, source_target_pairs={{32,0},{33,1},{34,2},{35,3},{36,4},{37,5},{38,6},{39,7},{40,8},{41... | collective-permute-start | bytes 6340616 | tf_op jit(solution)/shard_map/ppermute | solution.py:38
  258.4 57.6 %collective-permute-start.34 = (bf16[2064,512]{1,0:T(8,128)(2,1)}, bf16[2064,512]{1,0:T(8,128)(2,1)S(1)}, u32[]{:S(2)}, u32[]{:S(2)}) collective-permute-start(bf16[2064,512]{1,0:T(8,128)(2,1)} %get-tuple-element.23.refs_0_), channel_id=1, source_target_pairs={{96,0},{97,1},{98,2},{99,3},{100,4},{101,5},{102,6},{103,7},{104,8... | collective-permute-start | bytes 6340616 | tf_op jit(solution)/shard_map/ppermute | solution.py:38
  262.6 22.1 %collective-permute-start.25 = (f16[128,2176]{1,0:T(8,128)(2,1)S(1)}, f16[128,2176]{1,0:T(8,128)(2,1)S(1)}, u32[]{:S(2)}, u32[]{:S(2)}) collective-permute-start(f16[128,2176]{1,0:T(8,128)(2,1)S(1)} %get-tuple-element.42), channel_id=1, source_target_pairs={{1,0},{2,1},{3,2},{0,3},{5,4},{6,5},{7,6},{4,7},{9,8},{10,9},{11,1... | collective-permute-start | bytes 1671176 | tf_op jit(solution)/shard_map/ppermute | solution.py:38
  310.5 56.1 %collective-permute-start.42 = (bf16[2064,512]{1,0:T(8,128)(2,1)S(1)}, bf16[2064,512]{1,0:T(8,128)(2,1)}, u32[]{:S(2)}, u32[]{:S(2)}) collective-permute-start(bf16[2064,512]{1,0:T(8,128)(2,1)S(1)} %collective-permute-done.32.refs_0_), channel_id=1, source_target_pairs={{16,0},{17,1},{18,2},{19,3},{20,4},{21,5},{22,6},{23,7},{24,8},{25... | collective-permute-start | bytes 6340616 | tf_op jit(solution)/shard_map/ppermute | solution.py:38
  316.0 50.6 %collective-permute-start.43 = (bf16[2064,512]{1,0:T(8,128)(2,1)S(1)}, bf16[2064,512]{1,0:T(8,128)(2,1)}, u32[]{:S(2)}, u32[]{:S(2)}) collective-permute-start(bf16[2064,512]{1,0:T(8,128)(2,1)S(1)} %collective-permute-done.34.refs_3_), channel_id=1, source_target_pairs={{16,0},{17,1},{18,2},{19,3},{20,4},{21,5},{22,6},{23,7},{24,8},{25... | collective-permute-start | bytes 6340616 | tf_op jit(solution)/shard_map/ppermute | solution.py:38
  325.1 32.3 %collective-permute-start.33 = (bf16[1040,512]{1,0:T(8,128)(2,1)S(1)}, bf16[1040,512]{1,0:T(8,128)(2,1)S(1)}, u32[]{:S(2)}, u32[]{:S(2)}) collective-permute-start(bf16[1040,512]{1,0:T(8,128)(2,1)S(1)} %slice.170), channel_id=1, source_target_pairs={{32,0},{33,1},{34,2},{35,3},{36,4},{37,5},{38,6},{39,7},{40,8},{41... | collective-permute-start | bytes 3194888 | tf_op jit(solution)/shard_map/ppermute | solution.py:38
  328.3 25.4 %collective-permute-start.35 = (bf16[1024,512]{1,0:T(8,128)(2,1)S(1)}, bf16[1024,512]{1,0:T(8,128)(2,1)S(1)}, u32[]{:S(2)}, u32[]{:S(2)}) collective-permute-start(bf16[1024,512]{1,0:T(8,128)(2,1)S(1)} %slice.171), channel_id=1, source_target_pairs={{96,0},{97,1},{98,2},{99,3},{100,4},{101,5},{102,6},{103,7},{104,8... | collective-permute-start | bytes 3145736 | tf_op jit(solution)/shard_map/ppermute | solution.py:38
  353.6 28.6 %collective-permute-start.41 = (bf16[1024,512]{1,0:T(8,128)(2,1)S(1)}, bf16[1024,512]{1,0:T(8,128)(2,1)}, u32[]{:S(2)}, u32[]{:S(2)}) collective-permute-start(bf16[1024,512]{1,0:T(8,128)(2,1)S(1)} %collective-permute-done.35.refs_1_), channel_id=1, source_target_pairs={{16,0},{17,1},{18,2},{19,3},{20,4},{21,5},{22,6},{23,7},{24,8},{25... | collective-permute-start | bytes 3145736 | tf_op jit(solution)/shard_map/ppermute | solution.py:38
  357.4 24.8 %collective-permute-start.40 = (bf16[1040,512]{1,0:T(8,128)(2,1)S(1)}, bf16[1040,512]{1,0:T(8,128)(2,1)S(1)}, u32[]{:S(2)}, u32[]{:S(2)}) collective-permute-start(bf16[1040,512]{1,0:T(8,128)(2,1)S(1)} %collective-permute-done.33.refs_0_), channel_id=1, source_target_pairs={{16,0},{17,1},{18,2},{19,3},{20,4},{21,5},{22,6},{23,7},{24,8},{25... | collective-permute-start | bytes 3194888 | tf_op jit(solution)/shard_map/ppermute | solution.py:38
  (50 other events, 1135.6 us)
Sparse Core Ops, SparseCore 0:
  28.5 124.3 all-gather.1

commit v2 on v1

--- a/solution.py
+++ b/solution.py
@@ -65,60 +65,54 @@
 def forward_kernel(*refs):
     xs, ds, was, wbs = refs[:5], refs[5:10], refs[10:14], refs[14:18]
     acts, side, x_own, d_own = refs[18:22]
-    x, d, wa, wb, gate, up, back, act, sx, sd, sw, so = refs[22:]
+    v, w, sums, act, sx, sd, sw, so = refs[22:]
     z, y = place()
     x_copies, d_copies = [], []
     for i, first, count, off in FROM:
         for j in range(count):
             row = pl.multiple_of((lax.rem(z + first + j, 4) * 4 + lax.rem(y + off, 4)) * ROWS, ROWS)
             x_copies.append(
-                pltpu.make_async_copy(xs[i].at[pl.ds(j * ROWS, ROWS)], x.at[pl.ds(row, ROWS)], sx.at[len(x_copies)]))
+                pltpu.make_async_copy(xs[i].at[j], v.at[0, pl.ds(row, ROWS)], sx.at[len(x_copies)]))
             row = pl.multiple_of((lax.rem(z + off, 4) * 4 + lax.rem(y + first + j, 4)) * ROWS, ROWS)
             d_copies.append(
-                pltpu.make_async_copy(ds[i].at[pl.ds(j * ROWS, ROWS)], d.at[pl.ds(row, ROWS)], sd.at[len(d_copies)]))
+                pltpu.make_async_copy(ds[i].at[j], v.at[1, pl.ds(row, ROWS)], sd.at[len(d_copies)]))
+    rest = UNITS - CUT
     w_copies = [
-        [pltpu.make_async_copy(was[k], wa.at[k], sw.at[2 * k]), pltpu.make_async_copy(wbs[k], wb.at[k], sw.at[2 * k + 1])]
+        [
+            pltpu.make_async_copy(was[k].at[pl.ds(0, UNITS)], w.at[k, 0], sw.at[4 * k]),
+            pltpu.make_async_copy(wbs[k].at[pl.ds(0, UNITS)], w.at[k, 1], sw.at[4 * k + 1]),
+            pltpu.make_async_copy(was[k].at[pl.ds(UNITS, CUT)], w.at[k, 2, pl.ds(0, CUT)], sw.at[4 * k + 2]),
+            pltpu.make_async_copy(wbs[k].at[pl.ds(UNITS, rest)], w.at[k, 2, pl.ds(CUT, rest)], sw.at[4 * k + 3]),
+        ]
         for k in range(4)
     ]
-    stages = [x_copies + w_copies[0], d_copies, w_copies[1], w_copies[2], w_copies[3]]
+    stages = [x_copies + w_copies[0][:2], d_copies + w_copies[0][2:], w_copies[1], w_copies[2], w_copies[3]]
 
     def begin(n):
-        if n < len(stages):
-            for c in stages[n]:
-                c.start()
+        for c in stages[n]:
+            c.start()
 
     def end(n):
         for c in stages[n]:
             c.wait()
-
-    def first(k):
-        xk = x[:, k * DEPTH:(k + 1) * DEPTH]
-        for into, w in ((gate, wa), (up, wb)):
-            part = dot(w[k, :UNITS], xk, 1, 1)
-            into[...] = part if k == 0 else into[...] + part
-
-    def second(k):
-        dk = d[:, k * DEPTH:(k + 1) * DEPTH]
-        for rows, w in ((slice(0, CUT), wa), (slice(CUT, UNITS), wb)):
-            part = dot(w[k, UNITS:], dk, 1, 1)
-            back[rows, :] = part if k == 0 else back[rows, :] + part
 
     begin(0)
     begin(1)
     end(0)
     begin(2)
-    first(0)
+    for i in range(2):
+        sums[i] = dot(w[0, i], v[0, :, :DEPTH], 1, 1)
     end(1)
     begin(3)
-    second(0)
+    sums[2] = dot(w[0, 2], v[1, :, :DEPTH], 1, 1)
     end(2)
     begin(4)
     outs = []
-    for i, (v, to) in enumerate(((x, x_own), (d, d_own))):
-        outs.append(pltpu.make_async_copy(v.at[:, pl.ds(0, DEPTH)], to, so.at[i]))
+    for i, to in enumerate((x_own, d_own)):
+        outs.append(pltpu.make_async_copy(v.at[i, :, pl.ds(0, DEPTH)], to, so.at[i]))
         for h in range(2):
             outs.append(pltpu.make_async_copy(
-                v.at[:, pl.ds(DEPTH + h * TOK, TOK)],
+                v.at[i, :, pl.ds(DEPTH + h * TOK, TOK)],
                 side.at[pl.ds(3 * UNITS + (2 * i + h) * TOK, TOK)], so.at[2 + 2 * i + h]))
     for k in (1, 2, 3):
         if k > 1:
@@ -126,14 +120,18 @@
         if k == 3:
             for c in outs:
                 c.start()
-        first(k)
-        second(k)
+
+        def product(i, _):
+            sums[i] = sums[i] + dot(w[k, i], v[i // 2, :, k * DEPTH:(k + 1) * DEPTH], 1, 1)
+            return 0
+
+        lax.fori_loop(0, 3, product, 0)
 
     def unit(i, _):
         r = pl.ds(pl.multiple_of(i * 16, 16), 16)
-        g = gate[r, :].astype(BF).astype(F32)
-        u = up[r, :].astype(BF).astype(F32)
-        b = back[r, :].astype(BF).astype(F32)
+        g = sums[0, r, :].astype(BF).astype(F32)
+        u = sums[1, r, :].astype(BF).astype(F32)
+        b = sums[2, r, :].astype(BF).astype(F32)
         sigma = 1.0 / (1.0 + jnp.exp(-g))
         active = g * sigma
         act[r, :] = (b * u * sigma * (1.0 + g * (1.0 - sigma))).astype(BF)
@@ -156,12 +154,10 @@
         forward_kernel,
         (shape((3 * UNITS, TOK), BF), shape((3 * UNITS + 4 * TOK, TOK), BF), shape((TOK, DEPTH), BF), shape((TOK, DEPTH), BF)),
         [
-            pltpu.VMEM((TOK, WIDE), BF), pltpu.VMEM((TOK, WIDE), BF),
-            pltpu.VMEM((4, UNITS + CUT, DEPTH), BF), pltpu.VMEM((4, 2 * UNITS - CUT, DEPTH), BF),
-            pltpu.VMEM((UNITS, TOK), F32), pltpu.VMEM((UNITS, TOK), F32), pltpu.VMEM((UNITS, TOK), F32),
+            pltpu.VMEM((2, TOK, WIDE), BF), pltpu.VMEM((4, 3, UNITS, DEPTH), BF), pltpu.VMEM((3, UNITS, TOK), F32),
             pltpu.VMEM((3 * UNITS, TOK), BF),
             pltpu.SemaphoreType.DMA((16,)), pltpu.SemaphoreType.DMA((16,)),
-            pltpu.SemaphoreType.DMA((8,)), pltpu.SemaphoreType.DMA((8,)),
+            pltpu.SemaphoreType.DMA((16,)), pltpu.SemaphoreType.DMA((8,)),
         ],
         2 * TOK * WIDE * UNITS * 3,
         [ANY] * 18,
@@ -215,8 +211,14 @@
         if pending[k % 2]:
             for c in pending[k % 2]:
                 c.wait()
-        v = dot(tg[...], wa[k], 1, 0) + dot(tu[...], wb[k], 1, 0)
-        total[k % 2] = v * jnp.exp2(14.0 - expo[:, :1])
+
+        def tile(j, _):
+            n = pl.ds(pl.multiple_of(j * 512, 512), 512)
+            v = dot(tg[...], wa[k, :, n], 1, 0) + dot(tu[...], wb[k, :, n], 1, 0)
+            total[k % 2, :, n] = v * jnp.exp2(14.0 - expo[:, :1])
+            return 0
+
+        lax.fori_loop(0, 2, tile, 0)
         pending[k % 2] = puts(total.at[k % 2], k // 2, pl.ds((k % 2) * DEPTH, DEPTH), so.at[k % 2])
         for c in pending[k % 2]:
             c.start()
@@ -244,30 +246,29 @@
     )
 
 
-def join_kernel(*refs):
+def join_kernel(own_a, own_b, got, to_a, to_b):
     z, y = place()
-    for got, to, at in ((refs[0:4], refs[8], y), (refs[4:8], refs[9], z)):
+    for own, first, to, at in ((own_a, 0, to_a, y), (own_b, 3, to_b, z)):
         for s in range(4):
             r = pl.ds(pl.multiple_of(lax.rem(at + s, 4) * ROWS, ROWS), ROWS)
-            v = None
-            for g in got:
-                w = g[r, :HALF] * jnp.exp2(g[r, HALF:HALF + 1] - 14.0)
-                v = w if v is None else v + w
+            v = own[r, :HALF] * jnp.exp2(own[r, HALF:HALF + 1] - 14.0)
+            for i in range(first, first + 3):
+                v = v + got[i, r, :HALF] * jnp.exp2(got[i, r, HALF:HALF + 1] - 14.0)
             to[s] = v
 
 
-def joined(own_a, own_b, ra, rb):
+def joined(own_a, own_b, got):
     out = jax.ShapeDtypeStruct((4, ROWS, HALF), F32)
-    return call(
-        join_kernel, (out, out), [], 1 << 30, [VMEM] * 8, (VMEM,) * 2, (own_a, *ra, own_b, *rb), 12 << 20)
-
-
-def weight_kernel(picks, has_base, n_in, *refs):
+    return call(join_kernel, (out, out), [], 1 << 30, [VMEM] * 3, (VMEM,) * 2, (own_a, own_b, got), 12 << 20)
+
+
+def weight_kernel(acts, n_acts, columns, has_base, n_in, *refs):
     ins, outs = refs[:n_in], refs[n_in:n_in + 3]
     a, xc, dc, total, sa, sc, sb, so = refs[n_in + 3:]
+    z, y = place()
     stages = [[], [], []]
     n = 0
-    for g, (pieces, x_at, d_at) in enumerate(picks):
+    for g, pieces in enumerate(acts):
         for i, r0, r1 in pieces:
             for s in range(3):
                 lo, hi = max(r0, s * UNITS), min(r1, (s + 1) * UNITS)
@@ -275,15 +276,10 @@
                     stages[s].append(pltpu.make_async_copy(
                         ins[i].at[pl.ds(lo - r0, hi - lo)], a.at[pl.ds(lo, hi - lo), pl.ds(g * TOK, TOK)], sa.at[n]))
                     n += 1
-        for (i, sub), buf, s in ((x_at, xc, 0), (d_at, dc, 2)):
-            if len(ins[i].shape) == 4:
-                pairs = [(ins[i].at[:, sub], buf.at[g])]
-            elif sub is None:
-                pairs = [(ins[i], buf.at[g])]
-            else:
-                pairs = [(ins[i].at[pl.ds(sub + h * TOK, TOK)], buf.at[g, :, pl.ds(h * TOK, TOK)]) for h in range(2)]
-            for h, (src, to) in enumerate(pairs):
-                stages[s].append(pltpu.make_async_copy(src, to, sc.at[4 * g + s + h]))
+    columns(ins[n_acts:], z, y, lambda src, to: stages[0].append(
+        pltpu.make_async_copy(src, to, sc.at[0, len(stages[0])])), xc, 0)
+    columns(ins[n_acts:], z, y, lambda src, to: stages[2].append(
+        pltpu.make_async_copy(src, to, sc.at[1, len(stages[2])])), dc, 1)
     if has_base:
         for s in range(3):
             stages[s].append(pltpu.make_async_copy(ins[n_in - 3 + s], total.at[s], sb.at[s]))
@@ -301,7 +297,7 @@
         if i == 0:
             begin(2)
         cols = dc if i == 2 else xc
-        v = dot(a[i * UNITS:(i + 1) * UNITS, :], cols[...].reshape(len(picks) * TOK, DEPTH), 1, 0)
+        v = dot(a[i * UNITS:(i + 1) * UNITS, :], cols[...].reshape(len(acts) * TOK, DEPTH), 1, 0)
         total[i] = total[i] + v if has_base else v
         done.append(pltpu.make_async_copy(total.at[i], outs[i], so.at[i]))
         done[-1].start()
@@ -309,36 +305,43 @@
         c.wait()
 
 
-def weight_sums(groups, base):
-    ins, picks = [], []
-
-    def slot(v):
-        for i, w in enumerate(ins):
-            if w is v:
-                return i
-        ins.append(v)
-        return len(ins) - 1
-
-    n_pieces = 0
-    tiled = groups[0][2][0].ndim == 4
-    for pieces, rows, (xv, xi), (dv, di) in groups:
+def near_columns(refs, z, y, add, buf, kind):
+    x_own, d_own, side = refs[:3]
+    add(d_own if kind else x_own, buf.at[0])
+    for h in range(2):
+        add(side.at[pl.ds(3 * UNITS + (2 * kind + h) * TOK, TOK)], buf.at[1, :, pl.ds(h * TOK, TOK)])
+
+
+def plane_columns(first_group, count, refs, z, y, add, buf, kind):
+    for i, first, n, off in FROM:
+        for j in range(n):
+            a, b = lax.rem(z + first + j, 4), lax.rem(y + off, 4)
+            if kind:
+                a, b = lax.rem(z + off, 4), lax.rem(y + first + j, 4)
+            add(refs[5 * kind + i].at[j, pl.ds(first_group, count)], buf.at[:, a * 4 + b])
+
+
+def weight_sums(groups, columns, arrays, base):
+    ins, acts = [], []
+    for pieces in groups:
         row, marks = 0, []
-        for p, m in zip(pieces, rows):
-            marks.append((slot(p), row, row + m))
+        for p, m in pieces:
+            marks.append((len(ins), row, row + m))
+            ins.append(p)
             row += m
-            n_pieces += 1
-        picks.append((marks, (slot(xv), xi), (slot(dv), di)))
-    ins += list(base or [])
+        acts.append(marks)
+    n_acts = len(ins)
+    ins += list(arrays) + list(base or [])
     n = len(groups)
-    col = (n, 16, ROWS, DEPTH) if tiled else (n, TOK, DEPTH)
+    col = (n, TOK, DEPTH) if columns is near_columns else (n, 16, ROWS, DEPTH)
     out = jax.ShapeDtypeStruct((UNITS, DEPTH), F32)
     return call(
-        functools.partial(weight_kernel, picks, base is not None, len(ins)),
+        functools.partial(weight_kernel, acts, n_acts, columns, base is not None, len(ins)),
         (out,) * 3,
         [
             pltpu.VMEM((3 * UNITS, n * TOK), BF), pltpu.VMEM(col, BF), pltpu.VMEM(col, BF),
             pltpu.VMEM((3, UNITS, DEPTH), F32),
-            pltpu.SemaphoreType.DMA((3 * n_pieces,)), pltpu.SemaphoreType.DMA((4 * n,)),
+            pltpu.SemaphoreType.DMA((3 * n_acts,)), pltpu.SemaphoreType.DMA((2, 32)),
             pltpu.SemaphoreType.DMA((3,)), pltpu.SemaphoreType.DMA((3,)),
         ],
         2 * 3 * UNITS * DEPTH * n * TOK,
@@ -366,10 +369,11 @@
     x_own, d_own = jnp.concatenate(xp, axis=1), jnp.concatenate(dp, axis=1)
 
     def spread(own, first, second):
-        line = jnp.concatenate([own] + [moved(own, **{first: d}) for d in (1, 2, 3)], axis=0)
+        line = jnp.concatenate(
+            [own[None]] + [moved(own[None], **{first: d}) for d in (1, 2, 3)], axis=0)
         up, down = moved(line, **{second: 1}), moved(line, **{second: -1})
-        h = 2 * ROWS
-        return (line, up, down, moved(up[:h], **{second: 1}), moved(down[h:], **{second: -1}))
+        low, high = up[:2], down[2:]
+        return line, up, down, moved(low, **{second: 1}), moved(high, **{second: -1})
 
     xs = spread(x_own, "dz", "dy")
     ds = spread(d_own, "dy", "dz")
@@ -377,8 +381,9 @@
     side = moved(jnp.stack([xp[1], dp[1], xp[3], dp[3]]), flip=1)
     far = jnp.stack([xp[0], side[0], dp[0], side[1]])
     near = jnp.stack([xp[2], side[2], dp[2], side[3]])
-    got = jnp.stack([moved(near, dx=1), moved(near, dx=-1), moved(far, dx=2)])
-    cols = lax.all_gather(got.reshape(12, ROWS, DEPTH), "tp", axis=0)
+    got = (moved(near, dx=1), moved(near, dx=-1), moved(far, dx=2))
+    xcs = spread(jnp.concatenate([v[:2] for v in got], axis=0), "dz", "dy")
+    dcs = spread(jnp.concatenate([v[2:] for v in got], axis=0), "dy", "dz")
 
     wa = jnp.concatenate([w_gate.T, w_down[:CUT]], axis=0)
     wb = jnp.concatenate([w_up.T, w_down[CUT:]], axis=0)
@@ -391,28 +396,29 @@
 
     am, ap = moved(acts, dx=1), moved(acts, dx=-1)
     side = moved(side, flip=1)
-    oa, ob = moved(am[:LOW], dx=1), moved(ap[LOW:], dx=-1)
+    low, high = am[:LOW], ap[LOW:]
+    oa, ob = moved(low, dx=1), moved(high, dx=-1)
     sm, sp = moved(am, flip=1), moved(ap, flip=1)
     soa, sob = moved(oa, flip=1), moved(ob, flip=1)
 
     own_a, own_b, qa, qb = input_sums(acts, was, wbs)
     qa, qb = qa.astype(F16), qb.astype(F16)
-    ra = [moved(qa[d - 1], dz=-d).astype(F32) for d in (1, 2, 3)]
-    rb = [moved(qb[d - 1], dy=-d).astype(F32) for d in (1, 2, 3)]
-    fa, fb = joined(own_a, own_b, ra, rb)
+    got = [moved(qa[d - 1], dz=-d) for d in (1, 2, 3)] + [moved(qb[d - 1], dy=-d) for d in (1, 2, 3)]
+    got = jnp.stack(got).astype(F32)
+    fa, fb = joined(own_a, own_b, got)
     fa = fa[0] + moved(fa[1], dy=-1) + moved(fa[2], dy=-2) + moved(fa[3], dy=-3)
     fb = fb[0] + moved(fb[1], dz=-1) + moved(fb[2], dz=-2) + moved(fb[3], dz=-3)
     grad_inputs = jnp.concatenate(relative(jnp.concatenate([fa, fb], axis=1).astype(BF)), axis=1)
 
-    full, cut = (3 * UNITS,), (LOW, 3 * UNITS - LOW)
-    at = 3 * UNITS
+    full = 3 * UNITS
     sums = weight_sums(
-        [([acts], full, (x_cols, None), (d_cols, None)), ([side], full, (side, at), (side, at + 2 * TOK))], None)
+        [[(acts, full)], [(side, full)]], near_columns, (x_cols, d_cols, side), None)
     sums = weight_sums(
-        [([am], full, (cols, 0), (cols, 2)), ([sm], full, (cols, 1), (cols, 3)),
-         ([ap], full, (cols, 4), (cols, 6)), ([sp], full, (cols, 5), (cols, 7))], sums)
+        [[(am, full)], [(sm, full)], [(ap, full)], [(sp, full)]],
+        functools.partial(plane_columns, 0, 4), (*xcs, *dcs), sums)
     sums = weight_sums(
-        [([oa, ob], cut, (cols, 8), (cols, 10)), ([soa, sob], cut, (cols, 9), (cols, 11))], sums)
+        [[(oa, LOW), (ob, full - LOW)], [(soa, LOW), (sob, full - LOW)]],
+        functools.partial(plane_columns, 4, 2), (*xcs, *dcs), sums)
     return grad_inputs, sums[0].T, sums[1].T, sums[2]
 
 

time: 408 us -> 449 us (1.10)
  the two profiles are of different devices: /device:TPU:1 before, /device:TPU:0 now
where the time goes in v2:
time: 449 us; the launch traced here: 440 us
  waiting for transfers between devices  284 us (63%)
  Pallas kernels  73.9 us (16%)
  starting transfers between devices  54.3 us (12%)
  local copies, waits for them, and re-layouts  16.2 us (4%)
  other arithmetic  10.5 us (2%)
    ppermute x59, waiting for transfers between devices, moved(): return lax.ppermute(array, AXES, pairs)  284 us
    pallas_call x6, Pallas kernels, call(): pl.pallas_call(body, out_shape=out_shape, in_specs=ins, out_specs=outs, s...  73.9 us
    ppermute x59, starting transfers between devices, moved(): return lax.ppermute(array, AXES, pairs)  54.3 us
  transfers between devices with their start and end apart: 59, of which 28 were waited for; matrix products, arithmetic and copies ran while one was open for 4% of the time, Pallas kernels for 14%

profile of v2, /device:TPU:0, one launch (start us, length us, event | category | flops | bytes accessed | tf_op | source)
XLA Modules:
  0.0 440.3 jit_solution(1511814218331059867)
XLA Ops:
  43.0 7.5 %collective-permute-done.44 = bf16[1,6,32,1024]{3,2,1,0:T(8,128)(2,1)S(1)} collective-permute-done((bf16[1,6,32,1024]{3,2,1,0:T(8,128)(2,1)S(1)}, bf16[1,6,32,1024]{3,2,1,0:T(8,128)(2,1)S(1)}, u32[]{:S(2)}, u32[]{:S(2)}) %collective-permute-start.44) | collective-permute-done | bytes 393248 | tf_op jit(solution)/shard_map/ppermute | solution.py:38
  54.0 21.8 %collective-permute-done.51 = bf16[1,6,32,1024]{3,2,1,0:T(8,128)(2,1)S(1)} collective-permute-done((bf16[1,6,32,1024]{3,2,1,0:T(8,128)(2,1)S(1)}, bf16[1,6,32,1024]{3,2,1,0:T(8,128)(2,1)S(1)}, u32[]{:S(2)}, u32[]{:S(2)}) %collective-permute-start.51) | collective-permute-done | bytes 393248 | tf_op jit(solution)/shard_map/ppermute | solution.py:38
  76.3 7.6 %collective-permute-done.50 = bf16[1,6,32,1024]{3,2,1,0:T(8,128)(2,1)S(1)} collective-permute-done((bf16[1,6,32,1024]{3,2,1,0:T(8,128)(2,1)S(1)}, bf16[1,6,32,1024]{3,2,1,0:T(8,128)(2,1)S(1)}, u32[]{:S(2)}, u32[]{:S(2)}) %collective-permute-start.50) | collective-permute-done | bytes 393248 | tf_op jit(solution)/shard_map/ppermute | solution.py:38
  90.9 7.3 %collective-permute-done.10.refs_6_ = bf16[4,32,4096]{2,1,0:T(8,128)(2,1)S(1)} collective-permute-done((bf16[4,32,4096]{2,1,0:T(8,128)(2,1)S(1)}, bf16[4,32,4096]{2,1,0:T(8,128)(2,1)S(1)}, u32[]{:S(2)}, u32[]{:S(2)}) %collective-permute-start.10) | collective-permute-done | bytes 1048608 | tf_op jit(solution)/shard_map/ppermute | solution.py:38
  99.6 9.1 %collective-permute-done.11.refs_7_ = bf16[4,32,4096]{2,1,0:T(8,128)(2,1)S(1)} collective-permute-done((bf16[4,32,4096]{2,1,0:T(8,128)(2,1)S(1)}, bf16[4,32,4096]{2,1,0:T(8,128)(2,1)S(1)}, u32[]{:S(2)}, u32[]{:S(2)}) %collective-permute-start.11) | collective-permute-done | bytes 1048608 | tf_op jit(solution)/shard_map/ppermute | solution.py:38
  109.8 45.4 %collective-permute-done.6.refs_4_ = bf16[2,32,4096]{2,1,0:T(8,128)(2,1)S(1)} collective-permute-done((bf16[2,32,4096]{2,1,0:T(8,128)(2,1)S(1)}, bf16[2,32,4096]{2,1,0:T(8,128)(2,1)S(1)}, u32[]{:S(2)}, u32[]{:S(2)}) %collective-permute-start.6) | collective-permute-done | bytes 524320 | tf_op jit(solution)/shard_map/ppermute | solution.py:38
  155.2 10.7 %collective-permute-done.12.refs_8_ = bf16[2,32,4096]{2,1,0:T(8,128)(2,1)S(1)} collective-permute-done((bf16[2,32,4096]{2,1,0:T(8,128)(2,1)S(1)}, bf16[2,32,4096]{2,1,0:T(8,128)(2,1)S(1)}, u32[]{:S(2)}, u32[]{:S(2)}) %collective-permute-start.12) | collective-permute-done | bytes 524320 | tf_op jit(solution)/shard_map/ppermute | solution.py:38
  169.6 34.7 %collective-permute-done.52.refs_10_ = bf16[4,6,32,1024]{3,2,1,0:T(8,128)(2,1)S(1)} collective-permute-done((bf16[4,6,32,1024]{3,2,1,0:T(8,128)(2,1)S(1)}, bf16[4,6,32,1024]{3,2,1,0:T(8,128)(2,1)S(1)}, u32[]{:S(2)}, u32[]{:S(2)}) %collective-permute-start.52) | collective-permute-done | bytes 1572896 | tf_op jit(solution)/shard_map/ppermute | solution.py:38
  207.2 11.8 %collective-permute-done.13.refs_9_ = bf16[2,32,4096]{2,1,0:T(8,128)(2,1)S(1)} collective-permute-done((bf16[2,32,4096]{2,1,0:T(8,128)(2,1)S(1)}, bf16[2,32,4096]{2,1,0:T(8,128)(2,1)S(1)}, u32[]{:S(2)}, u32[]{:S(2)}) %collective-permute-start.13) | collective-permute-done | bytes 524320 | tf_op jit(solution)/shard_map/ppermute | solution.py:38
  223.8 19.0 %shard_map.84 = (bf16[2064,512]{1,0:T(8,128)(2,1)}, bf16[4112,512]{1,0:T(8,128)(2,1)}, bf16[512,1024]{1,0:T(8,128)(2,1)}, bf16[512,1024]{1,0:T(8,128)(2,1)}) custom-call(bf16[4,32,4096]{2,1,0:T(8,128)(2,1)} %copy-done.15, bf16[4,32,4096]{2,1,0:T(8,128)(2,1)} %copy-done.23, bf16[4,32,4096]{2,1,0:T(8,128)(2,1)} %copy-done.24, bf16[2,32,4096]{2,1,0:T(8,128)(2,1)} %copy-done.32, ...), custom_call_target="tpu_custom_call" | custom-call | flops 8657043456 | bytes 35651584 | tf_op jit(solution)/shard_map/pallas_call | solution.py:51
  242.8 13.8 %shard_map.85 = (f32[128,2176]{1,0:T(8,128)}, f32[128,2176]{1,0:T(8,128)}, f32[3,128,2176]{2,1,0:T(8,128)}, f32[3,128,2176]{2,1,0:T(8,128)}) custom-call(bf16[2064,512]{1,0:T(8,128)(2,1)} %get-tuple-element.23.refs_0_, bf16[1024,1024]{1,0:T(8,128)(2,1)} %copy-done.8, bf16[1024,1024]{1,0:T(8,128)(2,1)} %copy-done.30, bf16[1024,1024]{1,0:T(8,128)(2,1)} %copy-done.29, ...), custom_call_target="tpu_custom_call" | custom-call | flops 5771362304 | bytes 23068672 | tf_op jit(solution)/shard_map/pallas_call | solution.py:51
  264.3 10.7 %collective-permute-done.20 = f16[128,2176]{1,0:T(8,128)(2,1)S(1)} collective-permute-done((f16[128,2176]{1,0:T(8,128)(2,1)S(1)}, f16[128,2176]{1,0:T(8,128)(2,1)S(1)}, u32[]{:S(2)}, u32[]{:S(2)}) %collective-permute-start.20) | collective-permute-done | bytes 557088 | tf_op jit(solution)/shard_map/ppermute | solution.py:38
  277.8 8.2 %collective-permute-done.21 = f16[128,2176]{1,0:T(8,128)(2,1)S(1)} collective-permute-done((f16[128,2176]{1,0:T(8,128)(2,1)S(1)}, f16[128,2176]{1,0:T(8,128)(2,1)S(1)}, u32[]{:S(2)}, u32[]{:S(2)}) %collective-permute-start.21) | collective-permute-done | bytes 557088 | tf_op jit(solution)/shard_map/ppermute | solution.py:38
  291.4 11.0 %collective-permute-done.23 = f16[128,2176]{1,0:T(8,128)(2,1)S(1)} collective-permute-done((f16[128,2176]{1,0:T(8,128)(2,1)S(1)}, f16[128,2176]{1,0:T(8,128)(2,1)S(1)}, u32[]{:S(2)}, u32[]{:S(2)}) %collective-permute-start.23) | collective-permute-done | bytes 557088 | tf_op jit(solution)/shard_map/ppermute | solution.py:38
  303.2 7.6 %collective-permute-done.24 = f16[128,2176]{1,0:T(8,128)(2,1)S(1)} collective-permute-done((f16[128,2176]{1,0:T(8,128)(2,1)S(1)}, f16[128,2176]{1,0:T(8,128)(2,1)S(1)}, u32[]{:S(2)}, u32[]{:S(2)}) %collective-permute-start.24) | collective-permute-done | bytes 557088 | tf_op jit(solution)/shard_map/ppermute | solution.py:38
  326.1 10.2 %collective-permute-done.54.refs_12_ = bf16[2,6,32,1024]{3,2,1,0:T(8,128)(2,1)S(1)} collective-permute-done((bf16[2,6,32,1024]{3,2,1,0:T(8,128)(2,1)S(1)}, bf16[2,6,32,1024]{3,2,1,0:T(8,128)(2,1)S(1)}, u32[]{:S(2)}, u32[]{:S(2)}) %collective-permute-start.54) | collective-permute-done | bytes 786464 | tf_op jit(solution)/shard_map/ppermute | solution.py:38
  337.1 9.8 %collective-permute-done.30 = f32[32,2048]{1,0:T(8,128)S(1)} collective-permute-done((f32[32,2048]{1,0:T(8,128)S(1)}, f32[32,2048]{1,0:T(8,128)S(1)}, u32[]{:S(2)}, u32[]{:S(2)}) %collective-permute-start.30) | collective-permute-done | bytes 262176 | tf_op jit(solution)/shard_map/ppermute | solution.py:38
  350.8 8.9 %collective-permute-done.32.refs_0_ = bf16[2064,512]{1,0:T(8,128)(2,1)} collective-permute-done((bf16[2064,512]{1,0:T(8,128)(2,1)}, bf16[2064,512]{1,0:T(8,128)(2,1)}, u32[]{:S(2)}, u32[]{:S(2)}) %collective-permute-start.32) | collective-permute-done | bytes 2113568 | tf_op jit(solution)/shard_map/ppermute | solution.py:38
  366.7 7.5 %collective-permute-done.26 = f32[32,2048]{1,0:T(8,128)S(1)} collective-permute-done((f32[32,2048]{1,0:T(8,128)S(1)}, f32[32,2048]{1,0:T(8,128)S(1)}, u32[]{:S(2)}, u32[]{:S(2)}) %collective-permute-start.26) | collective-permute-done | bytes 262176 | tf_op jit(solution)/shard_map/ppermute | solution.py:38
  374.6 16.5 %collective-permute-done.35.refs_1_ = bf16[1024,512]{1,0:T(8,128)(2,1)S(1)} collective-permute-done((bf16[1024,512]{1,0:T(8,128)(2,1)S(1)}, bf16[1024,512]{1,0:T(8,128)(2,1)S(1)}, u32[]{:S(2)}, u32[]{:S(2)}) %collective-permute-start.35) | collective-permute-done | bytes 1048608 | tf_op jit(solution)/shard_map/ppermute | solution.py:38
  391.9 7.3 %collective-permute-done.33.refs_0_ = bf16[1040,512]{1,0:T(8,128)(2,1)S(1)} collective-permute-done((bf16[1040,512]{1,0:T(8,128)(2,1)S(1)}, bf16[1040,512]{1,0:T(8,128)(2,1)S(1)}, u32[]{:S(2)}, u32[]{:S(2)}) %collective-permute-start.33) | collective-permute-done | bytes 1064992 | tf_op jit(solution)/shard_map/ppermute | solution.py:38
  400.0 9.3 %shard_map.87 = (f32[688,1024]{1,0:T(8,128)}, f32[688,1024]{1,0:T(8,128)}, f32[688,1024]{1,0:T(8,128)}) custom-call(bf16[2064,512]{1,0:T(8,128)(2,1)} %get-tuple-element.23.refs_0_, bf16[4112,512]{1,0:T(8,128)(2,1)} %collective-permute-done.58.refs_1_.refs_4_, bf16[512,1024]{1,0:T(8,128)(2,1)} %get-tuple-element.31.refs_2_, ...), custom_call_target="tpu_custom_call" | custom-call | flops 4328521728 | bytes 25165824 | tf_op jit(solution)/shard_map/pallas_call | solution.py:51
  412.4 16.0 %shard_map.88 = (f32[688,1024]{1,0:T(8,128)}, f32[688,1024]{1,0:T(8,128)}, f32[688,1024]{1,0:T(8,128)}) custom-call(bf16[2064,512]{1,0:T(8,128)(2,1)} %collective-permute-done.32.refs_0_, bf16[2064,512]{1,0:T(8,128)(2,1)} %collective-permute-done.56.refs_1_, bf16[2064,512]{1,0:T(8,128)(2,1)} %collective-permute-done.34.refs_2_, ...), custom_call_target="tpu_custom_call" | custom-call | flops 8657043456 | bytes 33554432 | tf_op jit(solution)/shard_map/pallas_call | solution.py:51
  429.7 10.4 %shard_map.89 = (f32[688,1024]{1,0:T(8,128)}, f32[688,1024]{1,0:T(8,128)}, f32[688,1024]{1,0:T(8,128)}) custom-call(bf16[1040,512]{1,0:T(8,128)(2,1)} %copy-done.11, bf16[1024,512]{1,0:T(8,128)(2,1)} %copy-done.13, bf16[1040,512]{1,0:T(8,128)(2,1)} %copy-done.12, bf16[1024,512]{1,0:T(8,128)(2,1)} %copy-done.14, bf16[4,6,32,1024]{3,2,1,0:T(8,128)(2,1)} %copy-done, ...), custom_call_target="tpu_custom_call" | custom-call | flops 4328521728 | bytes 25165824 | tf_op jit(solution)/shard_map/pallas_call | solution.py:51
  (222 shorter events, 116.6 us)
Async XLA Ops:
  40.9 46.5 %collective-permute-start.3 = (bf16[4,32,4096]{2,1,0:T(8,128)(2,1)S(1)}, bf16[4,32,4096]{2,1,0:T(8,128)(2,1)S(1)}, u32[]{:S(2)}, u32[]{:S(2)}) collective-permute-start(bf16[4,32,4096]{2,1,0:T(8,128)(2,1)S(1)} %pad_maximum_fusion.4.refs_0_), channel_id=1, source_target_pairs={{1,0},{2,1},{3,2},{0,3},{5,4},{6,5},{7,6},{4,7},{9,8},{10,9},{11,1... | collective-permute-start | bytes 3145736 | tf_op jit(solution)/shard_map/ppermute | solution.py:38
  41.0 49.7 %collective-permute-start.4 = (bf16[4,32,4096]{2,1,0:T(8,128)(2,1)S(1)}, bf16[4,32,4096]{2,1,0:T(8,128)(2,1)S(1)}, u32[]{:S(2)}, u32[]{:S(2)}) collective-permute-start(bf16[4,32,4096]{2,1,0:T(8,128)(2,1)S(1)} %pad_maximum_fusion.4.refs_0_), channel_id=1, source_target_pairs={{3,0},{0,1},{1,2},{2,3},{7,4},{4,5},{5,6},{6,7},{11,8},{8,9},{9,10... | collective-permute-start | bytes 3145736 | tf_op jit(solution)/shard_map/ppermute | solution.py:38
  51.2 32.7 %collective-permute-start.50 = (bf16[1,6,32,1024]{3,2,1,0:T(8,128)(2,1)S(1)}, bf16[1,6,32,1024]{3,2,1,0:T(8,128)(2,1)S(1)}, u32[]{:S(2)}, u32[]{:S(2)}) collective-permute-start(bf16[1,6,32,1024]{3,2,1,0:T(8,128)(2,1)S(1)} %maximum_bitcast_fusion.1), channel_id=1, source_target_pairs={{2,0},{3,1},{0,2},{1,3},{6,4},{7,5},{4,6},{5,7},{10,8},{11,9},{8,1... | collective-permute-start | bytes 1179656 | tf_op jit(solution)/shard_map/ppermute | solution.py:38
  52.4 32.8 %collective-permute-start.49 = (bf16[1,6,32,1024]{3,2,1,0:T(8,128)(2,1)S(1)}, bf16[1,6,32,1024]{3,2,1,0:T(8,128)(2,1)S(1)}, u32[]{:S(2)}, u32[]{:S(2)}) collective-permute-start(bf16[1,6,32,1024]{3,2,1,0:T(8,128)(2,1)S(1)} %maximum_bitcast_fusion.1), channel_id=1, source_target_pairs={{1,0},{2,1},{3,2},{0,3},{5,4},{6,5},{7,6},{4,7},{9,8},{10,9},{11,1... | collective-permute-start | bytes 1179656 | tf_op jit(solution)/shard_map/ppermute | solution.py:38
  85.1 80.8 %collective-permute-start.18 = (bf16[1040,1024]{1,0:T(8,128)(2,1)S(1)}, bf16[1040,1024]{1,0:T(8,128)(2,1)S(1)}, u32[]{:S(2)}, u32[]{:S(2)}) collective-permute-start(bf16[1040,1024]{1,0:T(8,128)(2,1)S(1)} %pad_maximum_fusion.refs_14_.refs_5_), channel_id=1, source_target_pairs={{96,0},{97,1},{98,2},{99,3},{100,4},{101,5},{102,6},{103,7},{104,8... | collective-permute-start | bytes 6389768 | tf_op jit(solution)/shard_map/ppermute | solution.py:38
  87.4 80.0 %collective-permute-start.15 = (bf16[1024,1024]{1,0:T(8,128)(2,1)S(1)}, bf16[1024,1024]{1,0:T(8,128)(2,1)S(1)}, u32[]{:S(2)}, u32[]{:S(2)}) collective-permute-start(bf16[1024,1024]{1,0:T(8,128)(2,1)S(1)} %pad_maximum_fusion.1.refs_10_.refs_1_), channel_id=1, source_target_pairs={{32,0},{33,1},{34,2},{35,3},{36,4},{37,5},{38,6},{39,7},{40,8},{41... | collective-permute-start | bytes 6291464 | tf_op jit(solution)/shard_map/ppermute | solution.py:38
  98.3 70.7 %collective-permute-start.45 = (bf16[4,6,32,1024]{3,2,1,0:T(8,128)(2,1)S(1)}, bf16[4,6,32,1024]{3,2,1,0:T(8,128)(2,1)S(1)}, u32[]{:S(2)}, u32[]{:S(2)}) collective-permute-start(bf16[4,6,32,1024]{3,2,1,0:T(8,128)(2,1)S(1)} %pad_maximum_fusion.2.refs_4_), channel_id=1, source_target_pairs={{1,0},{2,1},{3,2},{0,3},{5,4},{6,5},{7,6},{4,7},{9,8},{10,9},{11,1... | collective-permute-start | bytes 4718600 | tf_op jit(solution)/shard_map/ppermute | solution.py:38
  108.7 60.5 %collective-permute-start.46 = (bf16[4,6,32,1024]{3,2,1,0:T(8,128)(2,1)S(1)}, bf16[4,6,32,1024]{3,2,1,0:T(8,128)(2,1)S(1)}, u32[]{:S(2)}, u32[]{:S(2)}) collective-permute-start(bf16[4,6,32,1024]{3,2,1,0:T(8,128)(2,1)S(1)} %pad_maximum_fusion.2.refs_4_), channel_id=1, source_target_pairs={{3,0},{0,1},{1,2},{2,3},{7,4},{4,5},{5,6},{6,7},{11,8},{8,9},{9,10... | collective-permute-start | bytes 4718600 | tf_op jit(solution)/shard_map/ppermute | solution.py:38
  108.8 46.4 %collective-permute-start.6 = (bf16[2,32,4096]{2,1,0:T(8,128)(2,1)S(1)}, bf16[2,32,4096]{2,1,0:T(8,128)(2,1)S(1)}, u32[]{:S(2)}, u32[]{:S(2)}) collective-permute-start(bf16[2,32,4096]{2,1,0:T(8,128)(2,1)S(1)} %slice.197), channel_id=1, source_target_pairs={{3,0},{0,1},{1,2},{2,3},{7,4},{4,5},{5,6},{6,7},{11,8},{8,9},{9,10... | collective-permute-start | bytes 1572872 | tf_op jit(solution)/shard_map/ppermute | solution.py:38
  165.9 53.2 %collective-permute-start.17 = (bf16[1040,1024]{1,0:T(8,128)(2,1)S(1)}, bf16[1040,1024]{1,0:T(8,128)(2,1)S(1)}, u32[]{:S(2)}, u32[]{:S(2)}) collective-permute-start(bf16[1040,1024]{1,0:T(8,128)(2,1)S(1)} %pad_maximum_fusion.refs_14_.refs_5_), channel_id=1, source_target_pairs={{16,0},{17,1},{18,2},{19,3},{20,4},{21,5},{22,6},{23,7},{24,8},{25... | collective-permute-start | bytes 6389768 | tf_op jit(solution)/shard_map/ppermute | solution.py:38
  166.7 57.1 %collective-permute-start.19 = (bf16[1040,1024]{1,0:T(8,128)(2,1)S(1)}, bf16[1040,1024]{1,0:T(8,128)(2,1)}, u32[]{:S(2)}, u32[]{:S(2)}) collective-permute-start(bf16[1040,1024]{1,0:T(8,128)(2,1)S(1)} %collective-permute-done.18.refs_16_.refs_7_), channel_id=1, source_target_pairs={{16,0},{17,1},{18,2},{19,3},{20,4},{21,5},{22,6},{23,7},{24,8},{25... | collective-permute-start | bytes 6389768 | tf_op jit(solution)/shard_map/ppermute | solution.py:38
  167.4 36.9 %collective-permute-start.52 = (bf16[4,6,32,1024]{3,2,1,0:T(8,128)(2,1)S(1)}, bf16[4,6,32,1024]{3,2,1,0:T(8,128)(2,1)S(1)}, u32[]{:S(2)}, u32[]{:S(2)}) collective-permute-start(bf16[4,6,32,1024]{3,2,1,0:T(8,128)(2,1)S(1)} %pad_maximum_fusion.3.refs_9_), channel_id=1, source_target_pairs={{4,0},{5,1},{6,2},{7,3},{8,4},{9,5},{10,6},{11,7},{12,8},{13,9},{1... | collective-permute-start | bytes 4718600 | tf_op jit(solution)/shard_map/ppermute | solution.py:38
  169.0 50.0 %collective-permute-start.14 = (bf16[1024,1024]{1,0:T(8,128)(2,1)S(1)}, bf16[1024,1024]{1,0:T(8,128)(2,1)S(1)}, u32[]{:S(2)}, u32[]{:S(2)}) collective-permute-start(bf16[1024,1024]{1,0:T(8,128)(2,1)S(1)} %pad_maximum_fusion.1.refs_10_.refs_1_), channel_id=1, source_target_pairs={{16,0},{17,1},{18,2},{19,3},{20,4},{21,5},{22,6},{23,7},{24,8},{25... | collective-permute-start | bytes 6291464 | tf_op jit(solution)/shard_map/ppermute | solution.py:38
  169.3 53.1 %collective-permute-start.16 = (bf16[1024,1024]{1,0:T(8,128)(2,1)S(1)}, bf16[1024,1024]{1,0:T(8,128)(2,1)S(1)}, u32[]{:S(2)}, u32[]{:S(2)}) collective-permute-start(bf16[1024,1024]{1,0:T(8,128)(2,1)S(1)} %collective-permute-done.15.refs_12_.refs_3_), channel_id=1, source_target_pairs={{16,0},{17,1},{18,2},{19,3},{20,4},{21,5},{22,6},{23,7},{24,8},{25... | collective-permute-start | bytes 6291464 | tf_op jit(solution)/shard_map/ppermute | solution.py:38
  218.9 92.0 %collective-permute-start.53 = (bf16[4,6,32,1024]{3,2,1,0:T(8,128)(2,1)S(1)}, bf16[4,6,32,1024]{3,2,1,0:T(8,128)(2,1)S(1)}, u32[]{:S(2)}, u32[]{:S(2)}) collective-permute-start(bf16[4,6,32,1024]{3,2,1,0:T(8,128)(2,1)S(1)} %pad_maximum_fusion.3.refs_9_), channel_id=1, source_target_pairs={{12,0},{13,1},{14,2},{15,3},{0,4},{1,5},{2,6},{3,7},{4,8},{5,9},{6... | collective-permute-start | bytes 4718600 | tf_op jit(solution)/shard_map/ppermute | solution.py:38
  219.0 97.5 %collective-permute-start.47 = (bf16[2,6,32,1024]{3,2,1,0:T(8,128)(2,1)}, bf16[2,6,32,1024]{3,2,1,0:T(8,128)(2,1)S(1)}, u32[]{:S(2)}, u32[]{:S(2)}) collective-permute-start(bf16[2,6,32,1024]{3,2,1,0:T(8,128)(2,1)} %slice.219), channel_id=1, source_target_pairs={{1,0},{2,1},{3,2},{0,3},{5,4},{6,5},{7,6},{4,7},{9,8},{10,9},{11,1... | collective-permute-start | bytes 2359304 | tf_op jit(solution)/shard_map/ppermute | solution.py:38
  220.5 102.8 %collective-permute-start.48 = (bf16[2,6,32,1024]{3,2,1,0:T(8,128)(2,1)}, bf16[2,6,32,1024]{3,2,1,0:T(8,128)(2,1)S(1)}, u32[]{:S(2)}, u32[]{:S(2)}) collective-permute-start(bf16[2,6,32,1024]{3,2,1,0:T(8,128)(2,1)} %slice.220), channel_id=1, source_target_pairs={{3,0},{0,1},{1,2},{2,3},{7,4},{4,5},{5,6},{6,7},{11,8},{8,9},{9,10... | collective-permute-start | bytes 2359304 | tf_op jit(solution)/shard_map/ppermute | solution.py:38
  310.8 88.5 %collective-permute-start.58 = (bf16[4112,512]{1,0:T(8,128)(2,1)}, bf16[4112,512]{1,0:T(8,128)(2,1)}, u32[]{:S(2)}, u32[]{:S(2)}) collective-permute-start(bf16[4112,512]{1,0:T(8,128)(2,1)} %get-tuple-element.30), channel_id=1, source_target_pairs={{16,0},{17,1},{18,2},{19,3},{20,4},{21,5},{22,6},{23,7},{24,8},{25... | collective-permute-start | bytes 12632072 | tf_op jit(solution)/shard_map/ppermute | solution.py:38
  311.0 48.8 %collective-permute-start.32 = (bf16[2064,512]{1,0:T(8,128)(2,1)}, bf16[2064,512]{1,0:T(8,128)(2,1)}, u32[]{:S(2)}, u32[]{:S(2)}) collective-permute-start(bf16[2064,512]{1,0:T(8,128)(2,1)} %get-tuple-element.23.refs_0_), channel_id=1, source_target_pairs={{32,0},{33,1},{34,2},{35,3},{36,4},{37,5},{38,6},{39,7},{40,8},{41... | collective-permute-start | bytes 6340616 | tf_op jit(solution)/shard_map/ppermute | solution.py:38
  313.2 49.6 %collective-permute-start.34 = (bf16[2064,512]{1,0:T(8,128)(2,1)}, bf16[2064,512]{1,0:T(8,128)(2,1)}, u32[]{:S(2)}, u32[]{:S(2)}) collective-permute-start(bf16[2064,512]{1,0:T(8,128)(2,1)} %get-tuple-element.23.refs_0_), channel_id=1, source_target_pairs={{96,0},{97,1},{98,2},{99,3},{100,4},{101,5},{102,6},{103,7},{104,8... | collective-permute-start | bytes 6340616 | tf_op jit(solution)/shard_map/ppermute | solution.py:38
  359.8 51.7 %collective-permute-start.56 = (bf16[2064,512]{1,0:T(8,128)(2,1)}, bf16[2064,512]{1,0:T(8,128)(2,1)}, u32[]{:S(2)}, u32[]{:S(2)}) collective-permute-start(bf16[2064,512]{1,0:T(8,128)(2,1)} %collective-permute-done.32.refs_0_), channel_id=1, source_target_pairs={{16,0},{17,1},{18,2},{19,3},{20,4},{21,5},{22,6},{23,7},{24,8},{25... | collective-permute-start | bytes 6340616 | tf_op jit(solution)/shard_map/ppermute | solution.py:38
  362.8 48.7 %collective-permute-start.57 = (bf16[2064,512]{1,0:T(8,128)(2,1)}, bf16[2064,512]{1,0:T(8,128)(2,1)}, u32[]{:S(2)}, u32[]{:S(2)}) collective-permute-start(bf16[2064,512]{1,0:T(8,128)(2,1)} %collective-permute-done.34.refs_2_), channel_id=1, source_target_pairs={{16,0},{17,1},{18,2},{19,3},{20,4},{21,5},{22,6},{23,7},{24,8},{25... | collective-permute-start | bytes 6340616 | tf_op jit(solution)/shard_map/ppermute | solution.py:38
  399.3 29.1 %collective-permute-start.37 = (bf16[1024,512]{1,0:T(8,128)(2,1)S(1)}, bf16[1024,512]{1,0:T(8,128)(2,1)S(1)}, u32[]{:S(2)}, u32[]{:S(2)}) collective-permute-start(bf16[1024,512]{1,0:T(8,128)(2,1)S(1)} %collective-permute-done.35.refs_1_), channel_id=1, source_target_pairs={{16,0},{17,1},{18,2},{19,3},{20,4},{21,5},{22,6},{23,7},{24,8},{25... | collective-permute-start | bytes 3145736 | tf_op jit(solution)/shard_map/ppermute | solution.py:38
  399.3 29.1 %collective-permute-start.36 = (bf16[1040,512]{1,0:T(8,128)(2,1)S(1)}, bf16[1040,512]{1,0:T(8,128)(2,1)S(1)}, u32[]{:S(2)}, u32[]{:S(2)}) collective-permute-start(bf16[1040,512]{1,0:T(8,128)(2,1)S(1)} %collective-permute-done.33.refs_0_), channel_id=1, source_target_pairs={{16,0},{17,1},{18,2},{19,3},{20,4},{21,5},{22,6},{23,7},{24,8},{25... | collective-permute-start | bytes 3194888 | tf_op jit(solution)/shard_map/ppermute | solution.py:38
  (73 other events, 1754.1 us)
